TPU v7x, 32 devices: a whole 2x2x4 slice. The times are simulated.
32 devices in a mesh: kv: 16 (over z, y, x), tp: 2 (over core).
Axes of the slice: x: 2, y: 2, z: 4, core: 2. Of those that a mesh axis runs over, the one named last changes fastest.
Arguments:
- tokens: bfloat16 [64, 4096], P(None, 'kv')
- lengths: int32 [16], replicated, may hold values from 1 to 4, 28 in all
- memory: float32 [16, 16, 128, 128], P('kv', 'tp'), may hold values from -0.6 to 0.6
- norm_gain: float32 [4096], P('kv'), may hold values from 0.1 to 1.9
- w_query: bfloat16 [4096, 2048], P('kv', 'tp'), may hold values from -0.09375 to 0.09375
- w_key: bfloat16 [4096, 2048], P('kv', 'tp'), may hold values from -0.09375 to 0.09375
- w_value: bfloat16 [4096, 2048], P('kv', 'tp'), may hold values from -0.09375 to 0.09375
- w_outgate: bfloat16 [4096, 2048], P('kv', 'tp'), may hold values from -0.09375 to 0.09375
- w_alpha: bfloat16 [4096, 16], P('kv'), may hold values from -0.09375 to 0.09375
- w_beta: bfloat16 [4096, 16], P('kv'), may hold values from -0.09375 to 0.09375
- decay_log: float32 [16], P('tp'), may hold values from -4 to 0.5
- decay_bias: float32 [16], P('tp'), may hold values from -1 to 1
- head_gain: float32 [128], replicated, may hold values from 0.1 to 1.9
- w_output: bfloat16 [2048, 4096], P('tp', 'kv'), may hold values from -0.125 to 0.125
- mlp_gain: float32 [4096], P('kv'), may hold values from 0.1 to 1.9
- w_gate: bfloat16 [4096, 11264], P('kv', 'tp'), may hold values from -0.09375 to 0.09375
- w_up: bfloat16 [4096, 11264], P('kv', 'tp'), may hold values from -0.09375 to 0.09375
- w_down: bfloat16 [11264, 4096], P('tp', 'kv'), may hold values from -0.0546875 to 0.0546875
Outputs:
- layer_out: bfloat16 [64, 4096], P(None, 'kv')
- new_memory: float32 [16, 16, 128, 128], P('kv', 'tp')
Inputs may be any that keep to these rules, and one draw needn't show every extreme that they name: How many of a sequence's 4 slots hold live tokens; the live ones come first; the lengths add up to seven quarters of 16, rounded down.
All inputs are finite; a program needn't handle non-finite values.
Results may differ from a plain program's by a relative error of at most 0.012.
Values may be sent and summed in bfloat16 or wider, within the bound.
A program may use at most 64 MiB of HBM per device.

v0:
```python
import jax
import jax.numpy as jnp
from jax import lax
from jax.experimental import pallas as pl
from jax.experimental.pallas import tpu as pltpu
from jax.sharding import PartitionSpec as P

D = 4096
DK = 128
DV = 128
NEW = 4


epsilon = 1e-06


def unit_rows(values):
    return values * lax.rsqrt(jnp.sum(values * values, axis=-1, keepdims=True) + epsilon)


def advance(memory, queries, key_rows, value_rows, decays, betas):
    outputs = []
    for step in range(queries.shape[1]):
        memory = jnp.exp(decays[:, step])[:, :, None, None] * memory
        predicted = jnp.einsum(
            "shde,shd->she", memory, key_rows[:, step], precision=lax.Precision.HIGHEST
        )
        correction = betas[:, step][:, :, None] * (value_rows[:, step] - predicted)
        memory = memory + key_rows[:, step][:, :, :, None] * correction[:, :, None, :]
        outputs.append(
            jnp.einsum("shde,shd->she", memory, queries[:, step], precision=lax.Precision.HIGHEST)
        )
    return (memory, jnp.stack(outputs, axis=1))


def per_device(
    tokens,
    lengths,
    memory,
    norm_gain,
    w_query,
    w_key,
    w_value,
    w_outgate,
    w_alpha,
    w_beta,
    decay_log,
    decay_bias,
    head_gain,
    w_output,
    mlp_gain,
    w_gate,
    w_up,
    w_down,
):
    total_rows = tokens.shape[0]
    kv_count = lax.axis_size("kv")
    kv_place = lax.axis_index("kv")
    tp_place = lax.axis_index("tp")
    own_rows = total_rows // kv_count
    seq_dev = memory.shape[0]
    heads_dev = memory.shape[1]
    token_f = tokens.astype(jnp.float32)
    squares = jnp.sum(token_f * token_f, axis=1)
    scaled = (token_f * norm_gain).astype(jnp.bfloat16)
    part_query = jnp.dot(scaled, w_query, preferred_element_type=jnp.float32)
    part_key = jnp.dot(scaled, w_key, preferred_element_type=jnp.float32)
    part_value = jnp.dot(scaled, w_value, preferred_element_type=jnp.float32)
    part_gate = jnp.dot(scaled, w_outgate, preferred_element_type=jnp.float32)
    part_alpha = jnp.dot(scaled, w_alpha, preferred_element_type=jnp.float32)
    part_beta = jnp.dot(scaled, w_beta, preferred_element_type=jnp.float32)
    all_squares = lax.psum(squares, "kv")
    sum_query, sum_key, sum_value, sum_gate, sum_alpha, sum_beta = (
        lax.psum_scatter(part_query, "kv", scatter_dimension=0, tiled=True),
        lax.psum_scatter(part_key, "kv", scatter_dimension=0, tiled=True),
        lax.psum_scatter(part_value, "kv", scatter_dimension=0, tiled=True),
        lax.psum_scatter(part_gate, "kv", scatter_dimension=0, tiled=True),
        lax.psum_scatter(part_alpha, "kv", scatter_dimension=0, tiled=True),
        lax.psum_scatter(part_beta, "kv", scatter_dimension=0, tiled=True),
    )
    own_squares = lax.dynamic_slice_in_dim(all_squares, kv_place * own_rows, own_rows)
    rstd = lax.rsqrt(own_squares / D + epsilon)[:, None]
    queries = (sum_query * rstd).astype(jnp.bfloat16)
    key_rows = (sum_key * rstd).astype(jnp.bfloat16)
    value_rows = (sum_value * rstd).astype(jnp.bfloat16)
    outgate = (sum_gate * rstd).astype(jnp.bfloat16)
    alphas = lax.dynamic_slice_in_dim(sum_alpha * rstd, tp_place * heads_dev, heads_dev, 1)
    beta_pre = lax.dynamic_slice_in_dim(sum_beta * rstd, tp_place * heads_dev, heads_dev, 1)
    own_lengths = lax.dynamic_slice_in_dim(lengths, kv_place * seq_dev, seq_dev)
    live = jnp.arange(NEW, dtype=jnp.int32)[None, :] < own_lengths[:, None]
    query_h = unit_rows(queries.astype(jnp.float32).reshape(seq_dev, NEW, heads_dev, DK)) * DK ** (
        -0.5
    )
    key_h = unit_rows(key_rows.astype(jnp.float32).reshape(seq_dev, NEW, heads_dev, DK))
    value_h = value_rows.astype(jnp.float32).reshape(seq_dev, NEW, heads_dev, DV)
    decays = -jnp.exp(decay_log) * jax.nn.softplus(alphas + decay_bias)
    decays = jnp.where(live[:, :, None], decays.reshape(seq_dev, NEW, heads_dev), 0.0)
    betas = jnp.where(
        live[:, :, None], jax.nn.sigmoid(beta_pre).reshape(seq_dev, NEW, heads_dev), 0.0
    )
    new_memory, attended = advance(memory, query_h, key_h, value_h, decays, betas)
    attended = attended * lax.rsqrt(jnp.mean(attended * attended, axis=-1, keepdims=True) + epsilon)
    gate_h = outgate.astype(jnp.float32).reshape(seq_dev, NEW, heads_dev, DV)
    mixed = (
        (attended * head_gain * jax.nn.silu(gate_h))
        .astype(jnp.bfloat16)
        .reshape(own_rows, heads_dev * DV)
    )
    attn_terms = jnp.dot(
        lax.all_gather(mixed, "kv", axis=0, tiled=True),
        w_output,
        preferred_element_type=jnp.float32,
    )
    attn_total = lax.psum(attn_terms, "tp")
    hidden = (token_f + attn_total).astype(jnp.bfloat16)
    hidden_f = hidden.astype(jnp.float32)
    hidden_squares = jnp.sum(hidden_f * hidden_f, axis=1)
    hscaled = (hidden_f * mlp_gain).astype(jnp.bfloat16)
    all_live = (jnp.arange(NEW, dtype=jnp.int32)[None, :] < lengths[:, None]).reshape(total_rows)
    part_gate_rows = jnp.dot(hscaled, w_gate, preferred_element_type=jnp.float32)
    part_up_rows = jnp.dot(hscaled, w_up, preferred_element_type=jnp.float32)
    gate_rows, up_rows, mlp_squares = lax.psum((part_gate_rows, part_up_rows, hidden_squares), "kv")
    rstd2 = lax.rsqrt(mlp_squares / D + epsilon)[:, None]
    active = (jax.nn.silu(gate_rows * rstd2) * (up_rows * rstd2)).astype(jnp.bfloat16)
    feed_terms = jnp.dot(active, w_down, preferred_element_type=jnp.float32)
    feed_total = lax.psum(feed_terms.astype(jnp.bfloat16), "tp").astype(jnp.float32)
    layer_out = jnp.where(all_live[:, None], hidden_f + feed_total, 0.0).astype(jnp.bfloat16)
    return (layer_out, new_memory)


F32 = jnp.float32
BF16 = jnp.bfloat16
HIGH = lax.Precision.HIGHEST
TILE = 128
GROUP = 8


def iota(shape, axis):
    return lax.broadcasted_iota(jnp.int32, shape, axis)


def dot(a, b, precision=None):
    return jnp.dot(a, b, preferred_element_type=F32, precision=precision)


def fused(
    lens,
    tokens,
    norm_gain,
    decay_log,
    decay_bias,
    head_gain,
    mlp_gain,
    w_alpha,
    w_beta,
    memory,
    w_query,
    w_key,
    w_value,
    w_outgate,
    w_output,
    w_gate,
    w_up,
    w_down,
    out,
    new_memory,
    v_mem,
    v_query,
    v_key,
    v_value,
    v_outgate,
    v_output,
    v_gate,
    v_up,
    v_down,
    proj_send,
    proj_recv,
    proj_part,
    proj_last,
    small_send,
    small_recv,
    rs_buf,
    xs_buf,
    kq_buf,
    r_buf,
    u_buf,
    a_buf,
    ab_buf,
    mix_buf,
    mix_all,
    tp_send,
    tp_recv,
    sq_send,
    sq_recv,
    gu_send,
    gu_recv,
    gu_part,
    gu_last,
    act_all,
    load_sem,
    send_sem,
    recv_sem,
    tp_sem,
):
    kv_count = mix_all.shape[0]
    me = lax.axis_index("kv")
    tp = lax.axis_index("tp")
    rows, width = tokens.shape
    heads = v_mem.shape[0]
    wide = heads * DV
    compact = tp_send.shape[1]
    groups = compact // GROUP
    zones = kv_count // groups
    chunk = gu_send.shape[2]
    total_width = width * kv_count

    barrier = pltpu.get_barrier_semaphore()

    @pl.loop(1, kv_count)
    def _(off):
        pl.semaphore_signal(
            barrier,
            inc=1,
            device_id={"kv": lax.rem(me + off, kv_count)},
            device_id_type=pl.DeviceIdType.MESH,
        )

    pl.semaphore_signal(
        barrier, inc=1, device_id={"tp": 1 - tp}, device_id_type=pl.DeviceIdType.MESH
    )
    pairs = [
        (w_query, v_query),
        (w_key, v_key),
        (w_value, v_value),
        (w_outgate, v_outgate),
        (memory, v_mem),
        (w_output, v_output),
        (w_gate, v_gate),
        (w_up, v_up),
        (w_down, v_down),
    ]
    loads = [pltpu.make_async_copy(a, b, load_sem.at[n]) for n, (a, b) in enumerate(pairs)]
    for load in loads[:4]:
        load.start()

    def remote(src, dst, phase, slot, partner, arrival):
        return pltpu.make_async_remote_copy(
            src_ref=src,
            dst_ref=dst,
            send_sem=send_sem.at[phase, slot],
            recv_sem=recv_sem.at[phase, arrival],
            device_id={"kv": partner},
            device_id_type=pl.DeviceIdType.MESH,
        )

    def tp_swap(phase, value):
        tp_send[phase] = value
        swap = pltpu.make_async_remote_copy(
            src_ref=tp_send.at[phase],
            dst_ref=tp_recv.at[phase],
            send_sem=tp_sem.at[phase, 0],
            recv_sem=tp_sem.at[phase, 1],
            device_id={"tp": 1 - tp},
            device_id_type=pl.DeviceIdType.MESH,
        )
        swap.start()
        swap.wait()
        return value + tp_recv[phase]

    all_rows = kv_count * 4 * NEW
    row = iota((all_rows, rows), 0)
    spread = jnp.where(
        iota((all_rows, rows), 1) == (row >> 4) * NEW + (row & 3), 1.0, 0.0
    ).astype(BF16)
    tok = tokens[...]
    scaled = (tok.astype(F32) * norm_gain[...]).astype(BF16)
    wide_tok = dot(spread, tok)
    wide_scaled = dot(spread, scaled)
    squares = jnp.sum(wide_tok * wide_tok, axis=1, keepdims=True)
    part_of = (iota((all_rows, width), 0) >> 2) & 3
    all_heads = w_alpha.shape[0]
    place = iota((TILE, all_heads), 0)
    head_of = iota((TILE, all_heads), 1)
    w_small = dot(jnp.where(place == head_of, 1.0, 0.0).astype(BF16), w_alpha[...]) + dot(
        jnp.where(place == head_of + all_heads, 1.0, 0.0).astype(BF16), w_beta[...]
    )
    small = lax.dot_general(
        wide_scaled.astype(BF16),
        w_small.astype(BF16),
        (((1,), (1,)), ((), ())),
        preferred_element_type=F32,
    )
    lane = iota((all_rows, TILE), 1)
    small = jnp.where(lane == 2 * all_heads, squares, small)
    small_send[...] = small.reshape(kv_count, 16, TILE)[:, :GROUP, :]
    masked = [jnp.where(part_of == p, wide_scaled, 0.0).astype(BF16) for p in range(4)]
    for load in loads[:4]:
        load.wait()
    for load in loads[4:]:
        load.start()
    half = wide // 2
    for c in range(2):
        cols = slice(c * half, (c + 1) * half)
        acc = dot(masked[0], v_query[:, cols])
        acc = acc + dot(masked[1], v_key[:, cols])
        acc = acc + dot(masked[2], v_value[:, cols])
        acc = acc + dot(masked[3], v_outgate[:, cols])
        proj_send[:, :, cols] = acc.astype(BF16).reshape(kv_count, 16, half)

    pl.semaphore_wait(barrier, kv_count)

    zone_me = me // groups
    group_me = lax.rem(me, groups)
    steps = [*range(1, zones), 0]
    side, odd = zone_me // 2, lax.rem(zone_me, 2)

    def zone_of(step):
        if zones != 4:
            return lax.rem(zone_me + step, zones)
        across = (1 - side) * 2
        return [zone_me, across + 1 - odd, across + odd, side * 2 + 1 - odd][step]

    def peer(g):
        return lax.rem(group_me + g, groups)

    def send_plane(send, recv, phase, zone):
        for g in range(1, groups):
            slab = zone * groups + peer(g)
            remote(
                send.at[slab],
                recv.at[zone * groups + group_me],
                phase,
                slab,
                zone_me * groups + peer(g),
                zone * groups + group_me,
            ).start()

    def sum_plane(send, recv, phase, zone):
        added = send[zone * groups + group_me].astype(F32)
        for g in range(1, groups):
            slab = zone * groups + peer(g)
            remote(send.at[slab], recv.at[slab], phase, slab, me, slab).wait_recv()
            added = added + recv[slab].astype(F32)
        return added

    def reduce_start(send, recv, part, last, phase):
        for step in steps[:-1]:
            zone = zone_of(step)
            part[zone] = sum_plane(send, recv, phase, zone).astype(BF16)
            remote(
                part.at[zone],
                last.at[zone_me],
                phase + 1,
                zone,
                zone * groups + group_me,
                zone_me,
            ).start()
        return sum_plane(send, recv, phase, zone_me)

    def reduce_end(added, part, last, phase):
        for step in steps[:-1][::-1]:
            zone = zone_of(step)
            remote(part.at[zone], last.at[zone], phase + 1, zone, me, zone).wait_recv()
            added = added + last[zone].astype(F32)
        return added

    @pl.loop(1, kv_count)
    def _(off):
        to = lax.rem(me + off, kv_count)
        remote(small_send.at[to], small_recv.at[me], 5, to, to, me).start()

    for step in steps:
        send_plane(proj_send, proj_recv, 0, zone_of(step))

    slots_wide = kv_count * heads * NEW
    shape_a = (1, rows)
    shape_b = (1, slots_wide)
    shape_c = (rows, compact)
    length_a = jnp.zeros(shape_a, jnp.int32)
    start_a = jnp.zeros(shape_a, jnp.int32)
    length_b = jnp.zeros(shape_b, jnp.int32)
    start_b = jnp.zeros(shape_b, jnp.int32)
    length_c = jnp.zeros(shape_c, jnp.int32)
    start_c = jnp.zeros(shape_c, jnp.int32)
    seq_a = iota(shape_a, 1) >> 2
    seq_b = iota(shape_b, 1) >> 5
    seq_c = iota(shape_c, 0) >> 2
    begin = jnp.int32(0)
    for s in range(kv_count):
        length_a = jnp.where(seq_a == s, lens[s], length_a)
        start_a = jnp.where(seq_a == s, begin, start_a)
        length_b = jnp.where(seq_b == s, lens[s], length_b)
        start_b = jnp.where(seq_b == s, begin, start_b)
        length_c = jnp.where(seq_c == s, lens[s], length_c)
        start_c = jnp.where(seq_c == s, begin, start_c)
        begin = begin + lens[s]
    slot_a = iota(shape_a, 1) & 3
    rank_a = jnp.where(slot_a < length_a, start_a + slot_a, -1)
    pack = jnp.where(rank_a == iota((compact, rows), 0), 1.0, 0.0).astype(BF16)
    slot_c = iota(shape_c, 0) & 3
    rank_c = jnp.where(slot_c < length_c, start_c + slot_c, -1)
    unpack = jnp.where(rank_c == iota(shape_c, 1), 1.0, 0.0).astype(BF16)
    slot_b = iota(shape_b, 1) & 3
    head_b = (iota(shape_b, 1) >> 2) & (heads - 1)
    rank_b = jnp.where(slot_b < length_b, head_b * compact + start_b + slot_b, -1)
    collect = jnp.where(rank_b == iota((heads * compact, slots_wide), 0), 1.0, 0.0).astype(BF16)
    tok_packed = dot(pack, tok)

    total = reduce_start(proj_send, proj_recv, proj_part, proj_last, 0)
    small = small_send[me]
    for off in range(1, kv_count):
        src = lax.rem(me + off, kv_count)
        remote(small_send.at[src], small_recv.at[src], 5, src, src, src).wait_recv()
        small = small + small_recv[src]
    small = small[:NEW]
    lane = iota((NEW, TILE), 1)
    mean_sq = jnp.sum(jnp.where(lane == 2 * all_heads, small, 0.0), axis=1, keepdims=True)
    rstd = lax.rsqrt(mean_sq / total_width + epsilon)
    rstd_wide = jnp.broadcast_to(rstd, (NEW, TILE))
    small = small * rstd
    ab_buf[0:4, :] = small
    for p in range(4):
        rs_buf[p * NEW : (p + 1) * NEW, :] = rstd_wide
    eye = iota((heads, heads), 0) == iota((heads, heads), 1)
    rate = jnp.sum(jnp.where(eye, jnp.exp(decay_log[...]), 0.0), axis=1, keepdims=True)
    bias = jnp.sum(jnp.where(eye, decay_bias[...], 0.0), axis=1, keepdims=True)
    pick = iota((heads, TILE), 1) - iota((heads, TILE), 0)
    own_length = jnp.full((heads, 1), lens[me], jnp.int32)
    decay, beta = [], []
    for t in range(NEW):
        line = ab_buf[t : t + 1, :]
        alpha = jnp.sum(jnp.where(pick == tp * heads, line, 0.0), axis=1, keepdims=True)
        write = jnp.sum(
            jnp.where(pick == tp * heads + all_heads, line, 0.0), axis=1, keepdims=True
        )
        x = alpha + bias
        soft = jnp.maximum(x, 0.0) + jnp.log1p(jnp.exp(-jnp.abs(x)))
        live = own_length > t
        decay.append(jnp.exp(jnp.where(live, -rate * soft, 0.0)))
        beta.append(jnp.where(live, jax.nn.sigmoid(write), 0.0))
    total = reduce_end(total, proj_part, proj_last, 0)
    scale = rs_buf[...]
    for h in range(heads):
        piece = total[:, h * DV : (h + 1) * DV] * scale
        xs_buf[h * 16 : (h + 1) * 16, :] = piece.astype(BF16).astype(F32)

    def slot_rows(ref, index, stride):
        return ref[pl.ds(index, heads, stride=stride), :]

    query, key_rows, value, gate = (
        [slot_rows(xs_buf, p * NEW + t, 16) for t in range(NEW)] for p in range(4)
    )
    query = [unit_rows(x) * DK ** (-0.5) for x in query]
    key_rows = [unit_rows(x) for x in key_rows]
    for t in range(NEW):
        kq_buf[pl.ds(t, heads, stride=8), :] = key_rows[t]
        kq_buf[pl.ds(NEW + t, heads, stride=8), :] = query[t]
    loads[4].wait()
    for h in range(heads):
        r_buf[h * 8 : (h + 1) * 8, :] = dot(kq_buf[h * 8 : (h + 1) * 8, :], v_mem[h], HIGH)
    seen_k = [slot_rows(r_buf, t, 8) for t in range(NEW)]
    seen_q = [slot_rows(r_buf, NEW + t, 8) for t in range(NEW)]

    def inner(a, b):
        return jnp.sum(a * b, axis=1, keepdims=True)

    corrections = []
    for t in range(NEW):
        for r in range(t, NEW):
            seen_k[r] = seen_k[r] * decay[t]
            seen_q[r] = seen_q[r] * decay[t]
        fix = beta[t] * (value[t] - seen_k[t])
        corrections.append(fix)
        for r in range(t, NEW):
            if r > t:
                seen_k[r] = seen_k[r] + inner(key_rows[t], key_rows[r]) * fix
            seen_q[r] = seen_q[r] + inner(key_rows[t], query[r]) * fix
    for t in range(NEW):
        o = seen_q[t]
        o = o * lax.rsqrt(jnp.mean(o * o, axis=1, keepdims=True) + epsilon)
        o = o * head_gain[...] * (gate[t] * jax.nn.sigmoid(gate[t]))
        mix_buf[pl.ds(t, heads, stride=NEW), :] = o
    mix_all[me] = mix_buf[...].astype(BF16)

    @pl.loop(1, kv_count)
    def _(off):
        to = lax.rem(me + off, kv_count)
        remote(mix_all.at[me], mix_all.at[me], 2, to, to, me).start()

    u_buf[...] = jnp.zeros_like(u_buf)
    after = jnp.ones((heads, 1), F32)
    for t in range(NEW - 1, -1, -1):
        u_buf[pl.ds(t, heads, stride=8), :] = corrections[t] * after
        after = after * decay[t]
    a_buf[...] = jnp.broadcast_to(after, (heads, TILE))
    for h in range(heads):
        outer = lax.dot_general(
            kq_buf[h * 8 : (h + 1) * 8, :],
            u_buf[h * 8 : (h + 1) * 8, :],
            (((0,), (0,)), ((), ())),
            precision=HIGH,
            preferred_element_type=F32,
        )
        v_mem[h] = v_mem[h] * a_buf[h : h + 1, :] + outer
    store = pltpu.make_async_copy(v_mem, new_memory, load_sem.at[len(pairs)])
    store.start()

    for off in range(1, kv_count):
        src = lax.rem(me + off, kv_count)
        remote(mix_all.at[src], mix_all.at[src], 2, src, src, src).wait_recv()
    gathered = mix_all[...].reshape(slots_wide, DV)
    packed = dot(collect, gathered).astype(BF16)
    loads[5].wait()
    packed = jnp.concatenate(
        [packed[h * compact : (h + 1) * compact, :] for h in range(heads)], axis=1
    )
    attended = tp_swap(0, dot(packed, v_output[...]))
    hidden = (tok_packed + attended).astype(BF16).astype(F32)
    squares = jnp.broadcast_to(
        jnp.sum(hidden * hidden, axis=1, keepdims=True), (compact, TILE)
    )
    sq_send[...] = squares.reshape(groups, GROUP, TILE)

    @pl.loop(1, kv_count)
    def _(off):
        to = lax.rem(me + off, kv_count)
        remote(sq_send.at[lax.rem(to, groups)], sq_recv.at[me], 6, to, to, me).start()

    hscaled = hidden * mlp_gain[...]
    blank = jnp.zeros((GROUP, width), F32)
    gate_rows, up_rows = [], []
    for g in range(groups):
        own = hscaled[g * GROUP : (g + 1) * GROUP, :]
        gate_rows += [own, blank]
        up_rows += [blank, own]
    gate_rows = jnp.concatenate(gate_rows, axis=0).astype(BF16)
    up_rows = jnp.concatenate(up_rows, axis=0).astype(BF16)
    loads[6].wait()
    loads[7].wait()
    for step in steps:
        zone = zone_of(step)
        cols = pl.ds(pl.multiple_of(zone * chunk, TILE), chunk)
        term = dot(gate_rows, v_gate[:, cols]) + dot(up_rows, v_up[:, cols])
        gu_send[pl.ds(zone * groups, groups)] = term.astype(BF16).reshape(
            groups, 2 * GROUP, chunk
        )
        send_plane(gu_send, gu_recv, 3, zone)
    both = reduce_start(gu_send, gu_recv, gu_part, gu_last, 3)
    mean_sq = sq_send[group_me]
    for off in range(1, kv_count):
        src = lax.rem(me + off, kv_count)
        remote(sq_send.at[0], sq_recv.at[src], 6, src, src, src).wait_recv()
        mean_sq = mean_sq + sq_recv[src]
    rstd2 = lax.rsqrt(mean_sq / total_width + epsilon)[:, :1]
    both = reduce_end(both, gu_part, gu_last, 3)
    gated = both[:GROUP] * rstd2
    active = gated * jax.nn.sigmoid(gated) * (both[GROUP:] * rstd2)
    act_all[me] = active.astype(BF16)

    def pass_on(zone, slot, partner):
        block = zone * groups + group_me
        remote(act_all.at[block], act_all.at[block], 7, slot, partner, block).start()

    def arrive(block):
        remote(act_all.at[block], act_all.at[block], 7, block, me, block).wait_recv()

    def forward(zone):
        for g in range(1, groups):
            pass_on(zone, zone * groups + peer(g), zone_me * groups + peer(g))

    for step in steps[:-1]:
        there = zone_of(step) * groups + group_me
        pass_on(zone_me, there, there)
    forward(zone_me)
    near_first = steps[::-1]
    for step in near_first[1:]:
        zone = zone_of(step)
        arrive(zone * groups + group_me)
        forward(zone)
    loads[8].wait()
    feed = jnp.zeros((compact, width), F32)
    for step in near_first:
        zone = zone_of(step)
        for g in range(1, groups):
            arrive(zone * groups + peer(g))
        part = act_all[pl.ds(zone * groups, groups)].astype(F32).reshape(compact, chunk)
        cols = pl.ds(pl.multiple_of(zone * chunk, TILE), chunk)
        feed = feed + dot(part.astype(BF16), v_down[cols, :])
    result = (hidden + tp_swap(1, feed)).astype(BF16)
    out[...] = dot(unpack, result).astype(BF16)

    store.wait()

    @pl.loop(1, kv_count)
    def _(off):
        to = lax.rem(me + off, kv_count)
        remote(mix_all.at[me], mix_all.at[me], 2, to, to, me).wait_send()
        remote(small_send.at[to], small_recv.at[me], 5, to, to, me).wait_send()
        remote(sq_send.at[0], sq_recv.at[me], 6, to, to, me).wait_send()
        remote(act_all.at[me], act_all.at[me], 7, to, to, me).wait_send()

    for step in steps:
        zone = zone_of(step)
        for g in range(1, groups):
            slab = zone * groups + peer(g)
            remote(proj_send.at[slab], proj_recv.at[slab], 0, slab, me, slab).wait_send()
            remote(gu_send.at[slab], gu_recv.at[slab], 3, slab, me, slab).wait_send()
        if step:
            remote(proj_part.at[zone], proj_last.at[zone], 1, zone, me, zone).wait_send()
            remote(gu_part.at[zone], gu_last.at[zone], 4, zone, me, zone).wait_send()


def fused_device(
    tokens,
    lengths,
    memory,
    norm_gain,
    w_query,
    w_key,
    w_value,
    w_outgate,
    w_alpha,
    w_beta,
    decay_log,
    decay_bias,
    head_gain,
    w_output,
    mlp_gain,
    w_gate,
    w_up,
    w_down,
):
    kv_count = lax.axis_size("kv")
    rows, width = tokens.shape
    heads = memory.shape[1]
    live_rows = (rows // NEW) * 7 // 4
    compact = -(-live_rows // 16) * 16
    groups = compact // GROUP
    zones = kv_count // groups
    chunk = w_gate.shape[1] // zones
    wide = heads * DV
    vmem = pl.BlockSpec(memory_space=pltpu.VMEM)
    far = pl.BlockSpec(memory_space=pl.ANY)
    out, state = pl.pallas_call(
        fused,
        out_shape=(
            jax.ShapeDtypeStruct((rows, width), BF16),
            jax.ShapeDtypeStruct(memory.shape[1:], F32),
        ),
        in_specs=[pl.BlockSpec(memory_space=pltpu.SMEM)] + [vmem] * 8 + [far] * 9,
        out_specs=(vmem, far),
        scratch_shapes=[
            pltpu.VMEM(memory.shape[1:], F32),
            pltpu.VMEM(w_query.shape, BF16),
            pltpu.VMEM(w_key.shape, BF16),
            pltpu.VMEM(w_value.shape, BF16),
            pltpu.VMEM(w_outgate.shape, BF16),
            pltpu.VMEM(w_output.shape, BF16),
            pltpu.VMEM(w_gate.shape, BF16),
            pltpu.VMEM(w_up.shape, BF16),
            pltpu.VMEM(w_down.shape, BF16),
            pltpu.VMEM((kv_count, 16, wide), BF16),
            pltpu.VMEM((kv_count, 16, wide), BF16),
            pltpu.VMEM((zones, 16, wide), BF16),
            pltpu.VMEM((zones, 16, wide), BF16),
            pltpu.VMEM((kv_count, GROUP, TILE), F32),
            pltpu.VMEM((kv_count, GROUP, TILE), F32),
            pltpu.VMEM((16, TILE), F32),
            pltpu.VMEM((heads * 16, TILE), F32),
            pltpu.VMEM((heads * 8, TILE), F32),
            pltpu.VMEM((heads * 8, TILE), F32),
            pltpu.VMEM((heads * 8, TILE), F32),
            pltpu.VMEM((heads, TILE), F32),
            pltpu.VMEM((16, TILE), F32),
            pltpu.VMEM((heads * NEW, TILE), F32),
            pltpu.VMEM((kv_count, heads * NEW, TILE), BF16),
            pltpu.VMEM((2, compact, width), F32),
            pltpu.VMEM((2, compact, width), F32),
            pltpu.VMEM((groups, GROUP, TILE), F32),
            pltpu.VMEM((kv_count, GROUP, TILE), F32),
            pltpu.VMEM((kv_count, 2 * GROUP, chunk), BF16),
            pltpu.VMEM((kv_count, 2 * GROUP, chunk), BF16),
            pltpu.VMEM((zones, 2 * GROUP, chunk), BF16),
            pltpu.VMEM((zones, 2 * GROUP, chunk), BF16),
            pltpu.VMEM((kv_count, GROUP, chunk), BF16),
            pltpu.SemaphoreType.DMA((10,)),
            pltpu.SemaphoreType.DMA((8, kv_count)),
            pltpu.SemaphoreType.DMA((8, kv_count)),
            pltpu.SemaphoreType.DMA((2, 2)),
        ],
        compiler_params=pltpu.CompilerParams(
            collective_id=0, has_side_effects=True, vmem_limit_bytes=67043328
        ),
    )(
        lengths,
        tokens,
        norm_gain.reshape(1, -1),
        decay_log.reshape(1, -1),
        decay_bias.reshape(1, -1),
        head_gain.reshape(1, -1),
        mlp_gain.reshape(1, -1),
        w_alpha.T,
        w_beta.T,
        memory.reshape(memory.shape[1:]),
        w_query,
        w_key,
        w_value,
        w_outgate,
        w_output,
        w_gate,
        w_up,
        w_down,
    )
    return out, state.reshape(memory.shape)


def fits(tokens, memory, w_gate):
    kv_count = lax.axis_size("kv")
    rows, width = tokens.shape
    live_rows = (rows // NEW) * 7 // 4
    groups = -(-live_rows // 16) * 16 // GROUP
    return (
        lax.axis_size("tp") == 2
        and memory.shape[0] == 1
        and memory.shape[1] == 8
        and rows == kv_count * NEW
        and rows % 16 == 0
        and width % TILE == 0
        and kv_count % groups == 0
        and w_gate.shape[1] % (kv_count // groups * TILE) == 0
    )


def layer(*arrays):
    if fits(arrays[0], arrays[2], arrays[15]):
        return fused_device(*arrays)
    return per_device(*arrays)


def solution(mesh):
    placed = (
        P(None, "kv"),
        P(),
        P("kv", "tp", None, None),
        P("kv"),
        P("kv", "tp"),
        P("kv", "tp"),
        P("kv", "tp"),
        P("kv", "tp"),
        P("kv", None),
        P("kv", None),
        P("tp"),
        P("tp"),
        P(),
        P("tp", "kv"),
        P("kv"),
        P("kv", "tp"),
        P("kv", "tp"),
        P("tp", "kv"),
    )
    return jax.shard_map(
        layer,
        mesh=mesh,
        in_specs=placed,
        out_specs=(P(None, "kv"), P("kv", "tp", None, None)),
        check_vma=False,
    )
```

profile of v0, /device:TPU:0, one launch (start us, length us, event | category | flops | bytes accessed | tf_op | source)
XLA Modules:
  0.0 54.2 jit_solution(12248185424427510538)
XLA Ops:
  0.6 50.3 %shard_map.185 = (bf16[64,256]{1,0:T(8,128)(2,1)}, f32[8,128,128]{2,1,0:T(8,128)}) custom-call(s32[16]{0:T(128)} %lens.1, bf16[64,256]{1,0:T(8,128)(2,1)} %tokens.1, f32[1,256]{1,0:T(1,128)} %bitcast.13, f32[1,8]{1,0:T(1,128)} %bitcast.15, f32[1,8]{1,0:T(1,128)} %bitcast.16, f32[1,128]{1,0:T(1,128)} %bitcast.17, f32[1,256]{1,0:T(1,128)} %bitcast.14, ...), custom_call_target="tpu_custom_call" | custom-call | tf_op jit(solution)/shard_map/pallas_call | solution.py:644
  50.9 1.4 %copy.22 = bf16[64,256]{1,0:T(8,128)(2,1)} copy(bf16[64,256]{1,0:T(8,128)(2,1)} %get-tuple-element.8) | data formatting | bytes 65536
  52.3 1.9 %copy.23 = f32[1,8,128,128]{3,2,1,0:T(8,128)} copy(f32[1,8,128,128]{3,2,1,0:T(8,128)} %bitcast.9) | data formatting | bytes 1048576
where the time goes:
time: 54.5 us; the launch traced here: 54.2 us
  Pallas kernels  50.3 us (92%)
  local copies, waits for them, and re-layouts  3.25 us (6%)
  between operations  0.65 us (1%)
    pallas_call x1, Pallas kernels, fused_device(): pl.pallas_call(fused, out_shape=(jax.ShapeDtypeStruct((rows, width), BF16...  50.3 us
    unnamed x2, local copies, waits for them, and re-layouts  3.25 us

commit v1 on v0

--- a/solution.py
+++ b/solution.py
@@ -144,15 +144,15 @@
 
 
 def fused(
-    lens,
-    tokens,
-    norm_gain,
-    decay_log,
-    decay_bias,
-    head_gain,
-    mlp_gain,
-    w_alpha,
-    w_beta,
+    lens_far,
+    tokens_far,
+    norm_far,
+    decay_log_far,
+    decay_bias_far,
+    head_far,
+    mlp_far,
+    alpha_far,
+    beta_far,
     memory,
     w_query,
     w_key,
@@ -163,15 +163,17 @@
     w_up,
     w_down,
     out,
-    new_memory,
     v_mem,
-    v_query,
-    v_key,
-    v_value,
-    v_outgate,
+    lens,
+    tokens,
+    norm_gain,
+    decay_in,
+    head_gain,
+    mlp_gain,
+    v_ab,
+    v_proj,
     v_output,
-    v_gate,
-    v_up,
+    v_gu,
     v_down,
     proj_send,
     proj_recv,
@@ -179,13 +181,14 @@
     proj_last,
     small_send,
     small_recv,
+    small_part,
+    small_last,
     rs_buf,
     xs_buf,
     kq_buf,
     r_buf,
     u_buf,
     a_buf,
-    ab_buf,
     mix_buf,
     mix_all,
     tp_send,
@@ -213,47 +216,75 @@
     zones = kv_count // groups
     chunk = gu_send.shape[2]
     total_width = width * kv_count
+    all_heads = v_ab.shape[1]
+    zone_me = me // groups
+    group_me = lax.rem(me, groups)
+    steps = [*range(1, zones), 0]
+    side, odd = zone_me // 2, lax.rem(zone_me, 2)
+
+    def zone_of(step):
+        if zones != 4:
+            return lax.rem(zone_me + step, zones)
+        across = (1 - side) * 2
+        return [zone_me, across + 1 - odd, across + odd, side * 2 + 1 - odd][step]
+
+    def peer(g):
+        return lax.rem(group_me + g, groups)
 
     barrier = pltpu.get_barrier_semaphore()
 
-    @pl.loop(1, kv_count)
-    def _(off):
+    def greet(**where):
         pl.semaphore_signal(
-            barrier,
-            inc=1,
-            device_id={"kv": lax.rem(me + off, kv_count)},
-            device_id_type=pl.DeviceIdType.MESH,
-        )
-
-    pl.semaphore_signal(
-        barrier, inc=1, device_id={"tp": 1 - tp}, device_id_type=pl.DeviceIdType.MESH
-    )
-    pairs = [
-        (w_query, v_query),
-        (w_key, v_key),
-        (w_value, v_value),
-        (w_outgate, v_outgate),
-        (memory, v_mem),
-        (w_output, v_output),
-        (w_gate, v_gate),
-        (w_up, v_up),
-        (w_down, v_down),
-    ]
-    loads = [pltpu.make_async_copy(a, b, load_sem.at[n]) for n, (a, b) in enumerate(pairs)]
-    for load in loads[:4]:
-        load.start()
-
-    def remote(src, dst, phase, slot, partner, arrival):
+            barrier, inc=1, device_id=where, device_id_type=pl.DeviceIdType.MESH
+        )
+
+    for g in range(1, groups):
+        greet(kv=zone_me * groups + peer(g))
+    for step in steps[:-1]:
+        greet(kv=zone_of(step) * groups + group_me)
+    greet(tp=1 - tp)
+
+    def load(src, dst, sem):
+        return pltpu.make_async_copy(src, dst, load_sem.at[sem])
+
+    half = wide // 2
+    halves = [slice(c * half, (c + 1) * half) for c in range(2)]
+    load(tokens_far, tokens, 0).start()
+    load(norm_far, norm_gain, 1).start()
+    load(alpha_far, v_ab.at[0], 2).start()
+    load(beta_far, v_ab.at[1], 2).start()
+    for c in range(2):
+        for p, weight in enumerate((w_query, w_key, w_value, w_outgate)):
+            load(weight.at[:, halves[c]], v_proj.at[p, :, halves[c]], 3 + c).start()
+    load(lens_far, lens, 5).start()
+    load(decay_log_far, decay_in.at[0], 6).start()
+    load(decay_bias_far, decay_in.at[1], 6).start()
+    load(head_far, head_gain, 7).start()
+    load(mlp_far, mlp_gain, 8).start()
+
+    def loaded(ref, sem):
+        load(ref, ref, sem).wait()
+
+    plane_sem, gu_sem, near_sem, far_sem = 0, zones, 2 * zones, 3 * zones
+    proj_sem, mlp_sem, mix_sem, small_sem, few_sem, sq_sem = range(4 * zones, 4 * zones + 6)
+
+    def remote(src, dst, sent, arrival, partner):
         return pltpu.make_async_remote_copy(
             src_ref=src,
             dst_ref=dst,
-            send_sem=send_sem.at[phase, slot],
-            recv_sem=recv_sem.at[phase, arrival],
+            send_sem=send_sem.at[sent],
+            recv_sem=recv_sem.at[arrival],
             device_id={"kv": partner},
             device_id_type=pl.DeviceIdType.MESH,
         )
 
-    def tp_swap(phase, value):
+    def arrived(ref, arrival):
+        remote(ref, ref, 0, arrival, me).wait_recv()
+
+    def left(ref, sent):
+        remote(ref, ref, sent, 0, me).wait_send()
+
+    def tp_swap(phase, value, meanwhile=None):
         tp_send[phase] = value
         swap = pltpu.make_async_remote_copy(
             src_ref=tp_send.at[phase],
@@ -264,114 +295,114 @@
             device_id_type=pl.DeviceIdType.MESH,
         )
         swap.start()
+        if meanwhile is not None:
+            meanwhile()
         swap.wait()
         return value + tp_recv[phase]
 
-    all_rows = kv_count * 4 * NEW
-    row = iota((all_rows, rows), 0)
+    packed_rows = kv_count * 2 * NEW
+    row = iota((packed_rows, rows), 0)
     spread = jnp.where(
-        iota((all_rows, rows), 1) == (row >> 4) * NEW + (row & 3), 1.0, 0.0
+        iota((packed_rows, rows), 1) == (row >> 3) * NEW + (row & 3), 1.0, 0.0
     ).astype(BF16)
+    seq_row = iota((kv_count, rows), 0)
+    seq_row = lax.rem(seq_row, zones) * groups + seq_row // zones
+    lane = iota((kv_count, TILE), 1)
+    place = iota((TILE, all_heads), 0) & (2 * all_heads - 1)
+    head_of = iota((TILE, all_heads), 1)
+    one_alpha = jnp.where(place == head_of, 1.0, 0.0).astype(BF16)
+    one_beta = jnp.where(place == head_of + all_heads, 1.0, 0.0).astype(BF16)
+    loaded(tokens, 0)
+    loaded(norm_gain, 1)
     tok = tokens[...]
     scaled = (tok.astype(F32) * norm_gain[...]).astype(BF16)
-    wide_tok = dot(spread, tok)
     wide_scaled = dot(spread, scaled)
-    squares = jnp.sum(wide_tok * wide_tok, axis=1, keepdims=True)
-    part_of = (iota((all_rows, width), 0) >> 2) & 3
-    all_heads = w_alpha.shape[0]
-    place = iota((TILE, all_heads), 0)
-    head_of = iota((TILE, all_heads), 1)
-    w_small = dot(jnp.where(place == head_of, 1.0, 0.0).astype(BF16), w_alpha[...]) + dot(
-        jnp.where(place == head_of + all_heads, 1.0, 0.0).astype(BF16), w_beta[...]
-    )
-    small = lax.dot_general(
-        wide_scaled.astype(BF16),
-        w_small.astype(BF16),
-        (((1,), (1,)), ((), ())),
-        preferred_element_type=F32,
-    )
-    lane = iota((all_rows, TILE), 1)
-    small = jnp.where(lane == 2 * all_heads, squares, small)
-    small_send[...] = small.reshape(kv_count, 16, TILE)[:, :GROUP, :]
-    masked = [jnp.where(part_of == p, wide_scaled, 0.0).astype(BF16) for p in range(4)]
-    for load in loads[:4]:
-        load.wait()
-    for load in loads[4:]:
-        load.start()
-    half = wide // 2
+    part_of = iota((packed_rows, width), 0) & 7
+    low = jnp.where(part_of < NEW, wide_scaled, 0.0).astype(BF16)
+    high = jnp.where(part_of >= NEW, wide_scaled, 0.0).astype(BF16)
+    loaded(v_ab, 2)
+    w_small = (dot(one_alpha, v_ab[0]) + dot(one_beta, v_ab[1])).astype(BF16)
+    small = jnp.zeros((kv_count, TILE), F32)
+    squares = jnp.zeros((kv_count, TILE), F32)
+    for t in range(NEW):
+        take = jnp.where(iota((kv_count, rows), 1) == seq_row * NEW + t, 1.0, 0.0).astype(BF16)
+        took = lax.dot_general(
+            dot(take, scaled).astype(BF16),
+            w_small,
+            (((1,), (1,)), ((), ())),
+            preferred_element_type=F32,
+        )
+        small = jnp.where(lane // (2 * all_heads) == t, took, small)
+        tok_t = dot(take, tok)
+        squares = jnp.where(
+            lane == t, jnp.sum(tok_t * tok_t, axis=1, keepdims=True), squares
+        )
+    small_send[:, :, 0, :] = small.reshape(groups, zones, TILE)
+    small_send[:, :, 1, :] = squares.reshape(groups, zones, TILE)
     for c in range(2):
-        cols = slice(c * half, (c + 1) * half)
-        acc = dot(masked[0], v_query[:, cols])
-        acc = acc + dot(masked[1], v_key[:, cols])
-        acc = acc + dot(masked[2], v_value[:, cols])
-        acc = acc + dot(masked[3], v_outgate[:, cols])
-        proj_send[:, :, cols] = acc.astype(BF16).reshape(kv_count, 16, half)
-
-    pl.semaphore_wait(barrier, kv_count)
-
-    zone_me = me // groups
-    group_me = lax.rem(me, groups)
-    steps = [*range(1, zones), 0]
-    side, odd = zone_me // 2, lax.rem(zone_me, 2)
-
-    def zone_of(step):
-        if zones != 4:
-            return lax.rem(zone_me + step, zones)
-        across = (1 - side) * 2
-        return [zone_me, across + 1 - odd, across + odd, side * 2 + 1 - odd][step]
-
-    def peer(g):
-        return lax.rem(group_me + g, groups)
-
-    def send_plane(send, recv, phase, zone):
+        loaded(v_proj.at[:, :, halves[c]], 3 + c)
+        parts = [
+            dot(low, v_proj[p, :, halves[c]]) + dot(high, v_proj[p + 1, :, halves[c]])
+            for p in (0, 2)
+        ]
+        parts = [part.reshape(kv_count, 2 * NEW, half) for part in parts]
+        proj_send[:, :, halves[c]] = jnp.concatenate(parts, axis=1).astype(BF16)
+    load(memory, v_mem, 9).start()
+    load(w_output, v_output, 10).start()
+    load(w_gate, v_gu.at[0], 11).start()
+    load(w_up, v_gu.at[1], 11).start()
+    load(w_down, v_down, 12).start()
+
+    pl.semaphore_wait(barrier, groups + zones - 1)
+
+    for g in range(1, groups):
+        remote(
+            small_send.at[peer(g)],
+            small_recv.at[group_me],
+            0,
+            small_sem,
+            zone_me * groups + peer(g),
+        ).start()
+
+    def send_plane(send, recv, sent, sem, zone):
         for g in range(1, groups):
-            slab = zone * groups + peer(g)
             remote(
-                send.at[slab],
+                send.at[zone * groups + peer(g)],
                 recv.at[zone * groups + group_me],
-                phase,
-                slab,
+                sent,
+                sem + zone,
                 zone_me * groups + peer(g),
-                zone * groups + group_me,
             ).start()
 
-    def sum_plane(send, recv, phase, zone):
+    def sum_plane(send, recv, sem, zone):
+        arrived(recv.at[pl.ds(zone * groups, groups - 1)], sem + zone)
         added = send[zone * groups + group_me].astype(F32)
         for g in range(1, groups):
-            slab = zone * groups + peer(g)
-            remote(send.at[slab], recv.at[slab], phase, slab, me, slab).wait_recv()
-            added = added + recv[slab].astype(F32)
+            added = added + recv[zone * groups + peer(g)].astype(F32)
         return added
 
-    def reduce_start(send, recv, part, last, phase):
+    def reduce_start(send, recv, part, last, sem, sent, arrival):
         for step in steps[:-1]:
             zone = zone_of(step)
-            part[zone] = sum_plane(send, recv, phase, zone).astype(BF16)
+            part[zone] = sum_plane(send, recv, sem, zone).astype(BF16)
             remote(
-                part.at[zone],
-                last.at[zone_me],
-                phase + 1,
-                zone,
-                zone * groups + group_me,
-                zone_me,
+                part.at[zone], last.at[zone_me], sent, arrival, zone * groups + group_me
             ).start()
-        return sum_plane(send, recv, phase, zone_me)
-
-    def reduce_end(added, part, last, phase):
-        for step in steps[:-1][::-1]:
-            zone = zone_of(step)
-            remote(part.at[zone], last.at[zone], phase + 1, zone, me, zone).wait_recv()
-            added = added + last[zone].astype(F32)
+        return sum_plane(send, recv, sem, zone_me)
+
+    def reduce_end(added, last, arrival):
+        arrived(last.at[pl.ds(0, zones - 1)], arrival)
+        for step in steps[:-1]:
+            added = added + last[zone_of(step)].astype(F32)
         return added
 
-    @pl.loop(1, kv_count)
-    def _(off):
-        to = lax.rem(me + off, kv_count)
-        remote(small_send.at[to], small_recv.at[me], 5, to, to, me).start()
-
     for step in steps:
-        send_plane(proj_send, proj_recv, 0, zone_of(step))
-
+        send_plane(proj_send, proj_recv, 1, plane_sem, zone_of(step))
+
+    loaded(lens, 5)
+    loaded(decay_in, 6)
+    loaded(head_gain, 7)
+    loaded(mlp_gain, 8)
     slots_wide = kv_count * heads * NEW
     shape_a = (1, rows)
     shape_b = (1, slots_wide)
@@ -406,39 +437,50 @@
     collect = jnp.where(rank_b == iota((heads * compact, slots_wide), 0), 1.0, 0.0).astype(BF16)
     tok_packed = dot(pack, tok)
 
-    total = reduce_start(proj_send, proj_recv, proj_part, proj_last, 0)
-    small = small_send[me]
-    for off in range(1, kv_count):
-        src = lax.rem(me + off, kv_count)
-        remote(small_send.at[src], small_recv.at[src], 5, src, src, src).wait_recv()
-        small = small + small_recv[src]
-    small = small[:NEW]
-    lane = iota((NEW, TILE), 1)
-    mean_sq = jnp.sum(jnp.where(lane == 2 * all_heads, small, 0.0), axis=1, keepdims=True)
+    arrived(small_recv.at[pl.ds(0, groups - 1)], small_sem)
+    small = small_send[group_me]
+    for g in range(1, groups):
+        small = small + small_recv[peer(g)]
+    small_part[...] = small
+    for step in steps[:-1]:
+        zone = zone_of(step)
+        remote(
+            small_part.at[zone], small_last.at[zone_me], 2, few_sem, zone * groups + group_me
+        ).start()
+
+    total = reduce_start(proj_send, proj_recv, proj_part, proj_last, plane_sem, 3, proj_sem)
+    arrived(small_last.at[pl.ds(0, zones - 1)], few_sem)
+    small = small_part[zone_me]
+    for step in steps[:-1]:
+        small = small + small_last[zone_of(step)]
+    diagonal = iota((NEW, TILE), 0) == iota((NEW, TILE), 1)
+    mean_sq = jnp.sum(jnp.where(diagonal, small[1:2, :], 0.0), axis=1, keepdims=True)
     rstd = lax.rsqrt(mean_sq / total_width + epsilon)
     rstd_wide = jnp.broadcast_to(rstd, (NEW, TILE))
-    small = small * rstd
-    ab_buf[0:4, :] = small
     for p in range(4):
         rs_buf[p * NEW : (p + 1) * NEW, :] = rstd_wide
     eye = iota((heads, heads), 0) == iota((heads, heads), 1)
-    rate = jnp.sum(jnp.where(eye, jnp.exp(decay_log[...]), 0.0), axis=1, keepdims=True)
-    bias = jnp.sum(jnp.where(eye, decay_bias[...], 0.0), axis=1, keepdims=True)
-    pick = iota((heads, TILE), 1) - iota((heads, TILE), 0)
+    rate = jnp.sum(jnp.where(eye, jnp.exp(decay_in[0]), 0.0), axis=1, keepdims=True)
+    bias = jnp.sum(jnp.where(eye, decay_in[1], 0.0), axis=1, keepdims=True)
+    pick = iota((heads, TILE), 1) - iota((heads, TILE), 0) - tp * heads
     own_length = jnp.full((heads, 1), lens[me], jnp.int32)
     decay, beta = [], []
     for t in range(NEW):
-        line = ab_buf[t : t + 1, :]
-        alpha = jnp.sum(jnp.where(pick == tp * heads, line, 0.0), axis=1, keepdims=True)
-        write = jnp.sum(
-            jnp.where(pick == tp * heads + all_heads, line, 0.0), axis=1, keepdims=True
+        line = small[0:1, :]
+        first = 2 * all_heads * t
+        scale_t = rstd[t : t + 1, :]
+        alpha = jnp.sum(jnp.where(pick == first, line, 0.0), axis=1, keepdims=True) * scale_t
+        write = (
+            jnp.sum(jnp.where(pick == first + all_heads, line, 0.0), axis=1, keepdims=True)
+            * scale_t
         )
         x = alpha + bias
         soft = jnp.maximum(x, 0.0) + jnp.log1p(jnp.exp(-jnp.abs(x)))
         live = own_length > t
         decay.append(jnp.exp(jnp.where(live, -rate * soft, 0.0)))
         beta.append(jnp.where(live, jax.nn.sigmoid(write), 0.0))
-    total = reduce_end(total, proj_part, proj_last, 0)
+    loaded(v_mem, 9)
+    total = reduce_end(total, proj_last, proj_sem)
     scale = rs_buf[...]
     for h in range(heads):
         piece = total[:, h * DV : (h + 1) * DV] * scale
@@ -455,7 +497,6 @@
     for t in range(NEW):
         kq_buf[pl.ds(t, heads, stride=8), :] = key_rows[t]
         kq_buf[pl.ds(NEW + t, heads, stride=8), :] = query[t]
-    loads[4].wait()
     for h in range(heads):
         r_buf[h * 8 : (h + 1) * 8, :] = dot(kq_buf[h * 8 : (h + 1) * 8, :], v_mem[h], HIGH)
     seen_k = [slot_rows(r_buf, t, 8) for t in range(NEW)]
@@ -485,7 +526,7 @@
     @pl.loop(1, kv_count)
     def _(off):
         to = lax.rem(me + off, kv_count)
-        remote(mix_all.at[me], mix_all.at[me], 2, to, to, me).start()
+        remote(mix_all.at[me], mix_all.at[me], 4, mix_sem, to).start()
 
     u_buf[...] = jnp.zeros_like(u_buf)
     after = jnp.ones((heads, 1), F32)
@@ -502,29 +543,28 @@
             preferred_element_type=F32,
         )
         v_mem[h] = v_mem[h] * a_buf[h : h + 1, :] + outer
-    store = pltpu.make_async_copy(v_mem, new_memory, load_sem.at[len(pairs)])
-    store.start()
-
-    for off in range(1, kv_count):
-        src = lax.rem(me + off, kv_count)
-        remote(mix_all.at[src], mix_all.at[src], 2, src, src, src).wait_recv()
+    loaded(v_output, 10)
+    loaded(v_gu, 11)
+    loaded(v_down, 12)
+
+    arrived(mix_all.at[pl.ds(0, kv_count - 1)], mix_sem)
     gathered = mix_all[...].reshape(slots_wide, DV)
     packed = dot(collect, gathered).astype(BF16)
-    loads[5].wait()
     packed = jnp.concatenate(
         [packed[h * compact : (h + 1) * compact, :] for h in range(heads)], axis=1
     )
     attended = tp_swap(0, dot(packed, v_output[...]))
     hidden = (tok_packed + attended).astype(BF16).astype(F32)
-    squares = jnp.broadcast_to(
-        jnp.sum(hidden * hidden, axis=1, keepdims=True), (compact, TILE)
-    )
-    sq_send[...] = squares.reshape(groups, GROUP, TILE)
+    squares = jnp.sum(hidden * hidden, axis=1, keepdims=True)
+    spot = (iota((compact, TILE), 0) & (GROUP - 1)) == iota((compact, TILE), 1)
+    squares = jnp.sum(jnp.where(spot, squares, 0.0).reshape(groups, GROUP, TILE), axis=1)
+    sq_send[...] = squares.reshape(groups, 1, TILE)
+    sq_recv[me] = sq_send[group_me]
 
     @pl.loop(1, kv_count)
     def _(off):
         to = lax.rem(me + off, kv_count)
-        remote(sq_send.at[lax.rem(to, groups)], sq_recv.at[me], 6, to, to, me).start()
+        remote(sq_send.at[lax.rem(to, groups)], sq_recv.at[me], 5, sq_sem, to).start()
 
     hscaled = hidden * mlp_gain[...]
     blank = jnp.zeros((GROUP, width), F32)
@@ -535,79 +575,62 @@
         up_rows += [blank, own]
     gate_rows = jnp.concatenate(gate_rows, axis=0).astype(BF16)
     up_rows = jnp.concatenate(up_rows, axis=0).astype(BF16)
-    loads[6].wait()
-    loads[7].wait()
     for step in steps:
         zone = zone_of(step)
         cols = pl.ds(pl.multiple_of(zone * chunk, TILE), chunk)
-        term = dot(gate_rows, v_gate[:, cols]) + dot(up_rows, v_up[:, cols])
+        term = dot(gate_rows, v_gu[0, :, cols]) + dot(up_rows, v_gu[1, :, cols])
         gu_send[pl.ds(zone * groups, groups)] = term.astype(BF16).reshape(
             groups, 2 * GROUP, chunk
         )
-        send_plane(gu_send, gu_recv, 3, zone)
-    both = reduce_start(gu_send, gu_recv, gu_part, gu_last, 3)
-    mean_sq = sq_send[group_me]
-    for off in range(1, kv_count):
-        src = lax.rem(me + off, kv_count)
-        remote(sq_send.at[0], sq_recv.at[src], 6, src, src, src).wait_recv()
-        mean_sq = mean_sq + sq_recv[src]
-    rstd2 = lax.rsqrt(mean_sq / total_width + epsilon)[:, :1]
-    both = reduce_end(both, gu_part, gu_last, 3)
+        send_plane(gu_send, gu_recv, 6, gu_sem, zone)
+    both = reduce_start(gu_send, gu_recv, gu_part, gu_last, gu_sem, 7, mlp_sem)
+    arrived(sq_recv.at[pl.ds(0, kv_count - 1)], sq_sem)
+    mean_sq = jnp.sum(sq_recv[...].reshape(kv_count, TILE), axis=0, keepdims=True)
+    spot = iota((GROUP, TILE), 0) == iota((GROUP, TILE), 1)
+    mean_sq = jnp.sum(jnp.where(spot, mean_sq, 0.0), axis=1, keepdims=True)
+    rstd2 = lax.rsqrt(mean_sq / total_width + epsilon)
+    both = reduce_end(both, gu_last, mlp_sem)
     gated = both[:GROUP] * rstd2
     active = gated * jax.nn.sigmoid(gated) * (both[GROUP:] * rstd2)
     act_all[me] = active.astype(BF16)
 
-    def pass_on(zone, slot, partner):
+    def pass_on(zone, arrival, partner):
         block = zone * groups + group_me
-        remote(act_all.at[block], act_all.at[block], 7, slot, partner, block).start()
-
-    def arrive(block):
-        remote(act_all.at[block], act_all.at[block], 7, block, me, block).wait_recv()
+        remote(act_all.at[block], act_all.at[block], 8, arrival, partner).start()
 
     def forward(zone):
         for g in range(1, groups):
-            pass_on(zone, zone * groups + peer(g), zone_me * groups + peer(g))
+            pass_on(zone, far_sem + zone, zone_me * groups + peer(g))
 
     for step in steps[:-1]:
-        there = zone_of(step) * groups + group_me
-        pass_on(zone_me, there, there)
+        pass_on(zone_me, near_sem + zone_me, zone_of(step) * groups + group_me)
     forward(zone_me)
     near_first = steps[::-1]
     for step in near_first[1:]:
         zone = zone_of(step)
-        arrive(zone * groups + group_me)
+        arrived(act_all.at[zone * groups + group_me], near_sem + zone)
         forward(zone)
-    loads[8].wait()
     feed = jnp.zeros((compact, width), F32)
     for step in near_first:
         zone = zone_of(step)
-        for g in range(1, groups):
-            arrive(zone * groups + peer(g))
+        arrived(act_all.at[pl.ds(zone * groups, groups - 1)], far_sem + zone)
         part = act_all[pl.ds(zone * groups, groups)].astype(F32).reshape(compact, chunk)
         cols = pl.ds(pl.multiple_of(zone * chunk, TILE), chunk)
         feed = feed + dot(part.astype(BF16), v_down[cols, :])
-    result = (hidden + tp_swap(1, feed)).astype(BF16)
+
+    def drain():
+        left(small_send.at[pl.ds(0, groups - 1)], 0)
+        left(proj_send.at[pl.ds(0, kv_count - zones)], 1)
+        left(small_part.at[pl.ds(0, zones - 1)], 2)
+        left(proj_part.at[pl.ds(0, zones - 1)], 3)
+        left(mix_all.at[pl.ds(0, kv_count - 1)], 4)
+        left(sq_recv.at[pl.ds(0, kv_count - 1)], 5)
+        left(gu_send.at[pl.ds(0, kv_count - zones)], 6)
+        left(gu_part.at[pl.ds(0, zones - 1)], 7)
+        left(act_all.at[pl.ds(0, kv_count - 1)], 8)
+
+    result = (hidden + tp_swap(1, feed, drain)).astype(BF16)
     out[...] = dot(unpack, result).astype(BF16)
-
-    store.wait()
-
-    @pl.loop(1, kv_count)
-    def _(off):
-        to = lax.rem(me + off, kv_count)
-        remote(mix_all.at[me], mix_all.at[me], 2, to, to, me).wait_send()
-        remote(small_send.at[to], small_recv.at[me], 5, to, to, me).wait_send()
-        remote(sq_send.at[0], sq_recv.at[me], 6, to, to, me).wait_send()
-        remote(act_all.at[me], act_all.at[me], 7, to, to, me).wait_send()
-
-    for step in steps:
-        zone = zone_of(step)
-        for g in range(1, groups):
-            slab = zone * groups + peer(g)
-            remote(proj_send.at[slab], proj_recv.at[slab], 0, slab, me, slab).wait_send()
-            remote(gu_send.at[slab], gu_recv.at[slab], 3, slab, me, slab).wait_send()
-        if step:
-            remote(proj_part.at[zone], proj_last.at[zone], 1, zone, me, zone).wait_send()
-            remote(gu_part.at[zone], gu_last.at[zone], 4, zone, me, zone).wait_send()
 
 
 def fused_device(
@@ -633,65 +656,69 @@
     kv_count = lax.axis_size("kv")
     rows, width = tokens.shape
     heads = memory.shape[1]
+    all_heads = w_alpha.shape[1]
     live_rows = (rows // NEW) * 7 // 4
     compact = -(-live_rows // 16) * 16
     groups = compact // GROUP
     zones = kv_count // groups
     chunk = w_gate.shape[1] // zones
     wide = heads * DV
-    vmem = pl.BlockSpec(memory_space=pltpu.VMEM)
-    far = pl.BlockSpec(memory_space=pl.ANY)
+    near = pl.BlockSpec(memory_space=pltpu.VMEM)
+    far = pl.BlockSpec(memory_space=pltpu.HBM)
     out, state = pl.pallas_call(
         fused,
         out_shape=(
             jax.ShapeDtypeStruct((rows, width), BF16),
             jax.ShapeDtypeStruct(memory.shape[1:], F32),
         ),
-        in_specs=[pl.BlockSpec(memory_space=pltpu.SMEM)] + [vmem] * 8 + [far] * 9,
-        out_specs=(vmem, far),
+        in_specs=[far] * 18,
+        out_specs=(near, near),
         scratch_shapes=[
-            pltpu.VMEM(memory.shape[1:], F32),
-            pltpu.VMEM(w_query.shape, BF16),
-            pltpu.VMEM(w_key.shape, BF16),
-            pltpu.VMEM(w_value.shape, BF16),
-            pltpu.VMEM(w_outgate.shape, BF16),
+            pltpu.SMEM(lengths.shape, jnp.int32),
+            pltpu.VMEM((rows, width), BF16),
+            pltpu.VMEM((1, width), F32),
+            pltpu.VMEM((2, 1, heads), F32),
+            pltpu.VMEM((1, DV), F32),
+            pltpu.VMEM((1, width), F32),
+            pltpu.VMEM((2, all_heads, width), BF16),
+            pltpu.VMEM((4, *w_query.shape), BF16),
             pltpu.VMEM(w_output.shape, BF16),
-            pltpu.VMEM(w_gate.shape, BF16),
-            pltpu.VMEM(w_up.shape, BF16),
+            pltpu.VMEM((2, *w_gate.shape), BF16),
             pltpu.VMEM(w_down.shape, BF16),
             pltpu.VMEM((kv_count, 16, wide), BF16),
             pltpu.VMEM((kv_count, 16, wide), BF16),
             pltpu.VMEM((zones, 16, wide), BF16),
             pltpu.VMEM((zones, 16, wide), BF16),
-            pltpu.VMEM((kv_count, GROUP, TILE), F32),
-            pltpu.VMEM((kv_count, GROUP, TILE), F32),
+            pltpu.VMEM((groups, zones, 2, TILE), F32),
+            pltpu.VMEM((groups, zones, 2, TILE), F32),
+            pltpu.VMEM((zones, 2, TILE), F32),
+            pltpu.VMEM((zones, 2, TILE), F32),
             pltpu.VMEM((16, TILE), F32),
             pltpu.VMEM((heads * 16, TILE), F32),
             pltpu.VMEM((heads * 8, TILE), F32),
             pltpu.VMEM((heads * 8, TILE), F32),
             pltpu.VMEM((heads * 8, TILE), F32),
             pltpu.VMEM((heads, TILE), F32),
-            pltpu.VMEM((16, TILE), F32),
             pltpu.VMEM((heads * NEW, TILE), F32),
             pltpu.VMEM((kv_count, heads * NEW, TILE), BF16),
             pltpu.VMEM((2, compact, width), F32),
             pltpu.VMEM((2, compact, width), F32),
-            pltpu.VMEM((groups, GROUP, TILE), F32),
-            pltpu.VMEM((kv_count, GROUP, TILE), F32),
+            pltpu.VMEM((groups, 1, TILE), F32),
+            pltpu.VMEM((kv_count, 1, TILE), F32),
             pltpu.VMEM((kv_count, 2 * GROUP, chunk), BF16),
             pltpu.VMEM((kv_count, 2 * GROUP, chunk), BF16),
             pltpu.VMEM((zones, 2 * GROUP, chunk), BF16),
             pltpu.VMEM((zones, 2 * GROUP, chunk), BF16),
             pltpu.VMEM((kv_count, GROUP, chunk), BF16),
-            pltpu.SemaphoreType.DMA((10,)),
-            pltpu.SemaphoreType.DMA((8, kv_count)),
-            pltpu.SemaphoreType.DMA((8, kv_count)),
+            pltpu.SemaphoreType.DMA((13,)),
+            pltpu.SemaphoreType.DMA((9,)),
+            pltpu.SemaphoreType.DMA((4 * zones + 6,)),
             pltpu.SemaphoreType.DMA((2, 2)),
         ],
         compiler_params=pltpu.CompilerParams(
-            collective_id=0, has_side_effects=True, vmem_limit_bytes=67043328
+            collective_id=0, has_side_effects=True, vmem_limit_bytes=48 * 1024 * 1024
         ),
-    )(
+    )(*[pltpu.with_memory_space_constraint(x, pltpu.HBM) for x in (
         lengths,
         tokens,
         norm_gain.reshape(1, -1),
@@ -710,15 +737,16 @@
         w_gate,
         w_up,
         w_down,
-    )
+    )])
     return out, state.reshape(memory.shape)
 
 
-def fits(tokens, memory, w_gate):
+def fits(tokens, memory, w_alpha, w_gate):
     kv_count = lax.axis_size("kv")
     rows, width = tokens.shape
     live_rows = (rows // NEW) * 7 // 4
     groups = -(-live_rows // 16) * 16 // GROUP
+    all_heads = w_alpha.shape[1]
     return (
         lax.axis_size("tp") == 2
         and memory.shape[0] == 1
@@ -728,11 +756,12 @@
         and width % TILE == 0
         and kv_count % groups == 0
         and w_gate.shape[1] % (kv_count // groups * TILE) == 0
+        and NEW * 2 * all_heads == TILE
     )
 
 
 def layer(*arrays):
-    if fits(arrays[0], arrays[2], arrays[15]):
+    if fits(arrays[0], arrays[2], arrays[8], arrays[15]):
         return fused_device(*arrays)
     return per_device(*arrays)
 

time: 54.5 us -> 46.8 us (0.86)
  Pallas kernels: 50.3 us -> 44.6 us
  local copies, waits for them, and re-layouts: 3.25 us -> 1.41 us
    pallas_call x1, Pallas kernels: 50.3 us -> 44.6 us  [fused_device(): pl.pallas_call(fused, out_shape=(jax.ShapeDtypeStruct((rows, width), BF16...]
    unnamed x2, local copies, waits for them, and re-layouts: 3.25 us -> 1.41 us
where the time goes in v1:
time: 46.8 us; the launch traced here: 46.7 us
  Pallas kernels  44.6 us (95%)
  local copies, waits for them, and re-layouts  1.41 us (3%)
  between operations  0.65 us (1%)
    pallas_call x1, Pallas kernels, fused_device(): pl.pallas_call(fused, out_shape=(jax.ShapeDtypeStruct((rows, width), BF16...  44.6 us
    unnamed x2, local copies, waits for them, and re-layouts  1.41 us

profile of v1, /device:TPU:0, one launch (start us, length us, event | category | flops | bytes accessed | tf_op | source)
XLA Modules:
  0.0 46.7 jit_solution(5347809757140968009)
XLA Ops:
  0.6 44.6 %shard_map.185 = (bf16[64,256]{1,0:T(8,128)(2,1)S(1)}, f32[8,128,128]{2,1,0:T(8,128)S(1)}) custom-call(s32[16]{0:T(128)} %lens_far.1, bf16[64,256]{1,0:T(8,128)(2,1)} %tokens_far.1, f32[1,256]{1,0:T(1,128)} %bitcast.13, f32[1,8]{1,0:T(1,128)} %bitcast.15, f32[1,8]{1,0:T(1,128)} %bitcast.16, f32[1,128]{1,0:T(1,128)} %bitcast.17, f32[1,256]{1,0:T(1,128)} %bitcast.14, ...), custom_call_target="tpu_custom_call" | custom-call | tf_op jit(solution)/shard_map/pallas_call | solution.py:668
  45.3 0.6 %copy.22 = bf16[64,256]{1,0:T(8,128)(2,1)} copy(bf16[64,256]{1,0:T(8,128)(2,1)S(1)} %get-tuple-element.8) | data formatting | bytes 65536
  45.9 0.8 %copy.23 = f32[1,8,128,128]{3,2,1,0:T(8,128)} copy(f32[1,8,128,128]{3,2,1,0:T(8,128)S(1)} %bitcast.9) | data formatting | bytes 1048576

commit v2 on v1

--- a/solution.py
+++ b/solution.py
@@ -214,7 +214,9 @@
     compact = tp_send.shape[1]
     groups = compact // GROUP
     zones = kv_count // groups
-    chunk = gu_send.shape[2]
+    sent = gu_send.shape[2]
+    chunk = sent + TILE
+    held = GROUP - 1
     total_width = width * kv_count
     all_heads = v_ab.shape[1]
     zone_me = me // groups
@@ -229,7 +231,15 @@
         return [zone_me, across + 1 - odd, across + odd, side * 2 + 1 - odd][step]
 
     def peer(g):
-        return lax.rem(group_me + g, groups)
+        if groups != 4:
+            return lax.rem(group_me + g, groups)
+        row, col = group_me // 2, lax.rem(group_me, 2)
+        return [
+            group_me,
+            (1 - row) * 2 + 1 - col,
+            row * 2 + 1 - col,
+            (1 - row) * 2 + col,
+        ][g]
 
     barrier = pltpu.get_barrier_semaphore()
 
@@ -238,10 +248,11 @@
             barrier, inc=1, device_id=where, device_id_type=pl.DeviceIdType.MESH
         )
 
-    for g in range(1, groups):
-        greet(kv=zone_me * groups + peer(g))
-    for step in steps[:-1]:
-        greet(kv=zone_of(step) * groups + group_me)
+    for core in (tp, 1 - tp):
+        for g in range(1, groups):
+            greet(kv=zone_me * groups + peer(g), tp=core)
+        for step in steps[:-1]:
+            greet(kv=zone_of(step) * groups + group_me, tp=core)
     greet(tp=1 - tp)
 
     def load(src, dst, sem):
@@ -265,16 +276,17 @@
     def loaded(ref, sem):
         load(ref, ref, sem).wait()
 
-    plane_sem, gu_sem, near_sem, far_sem = 0, zones, 2 * zones, 3 * zones
-    proj_sem, mlp_sem, mix_sem, small_sem, few_sem, sq_sem = range(4 * zones, 4 * zones + 6)
-
-    def remote(src, dst, sent, arrival, partner):
+    plane_sem, gu_sem, near_sem, far_sem = 0, zones, 3 * zones, 5 * zones
+    proj_sem, mlp_sem, mix_sem, small_sem, few_sem, sq_sem = range(6 * zones, 6 * zones + 6)
+    both_sem = 6 * zones + 6
+
+    def remote(src, dst, sent, arrival, partner, core=None):
         return pltpu.make_async_remote_copy(
             src_ref=src,
             dst_ref=dst,
             send_sem=send_sem.at[sent],
             recv_sem=recv_sem.at[arrival],
-            device_id={"kv": partner},
+            device_id={"kv": partner, "tp": tp if core is None else core},
             device_id_type=pl.DeviceIdType.MESH,
         )
 
@@ -320,6 +332,50 @@
     part_of = iota((packed_rows, width), 0) & 7
     low = jnp.where(part_of < NEW, wide_scaled, 0.0).astype(BF16)
     high = jnp.where(part_of >= NEW, wide_scaled, 0.0).astype(BF16)
+
+    def sum_plane(recv, sem, first, own):
+        count = groups if own is None else groups - 1
+        arrived(recv.at[pl.ds(first, count)], sem)
+        added = (recv[first + group_me] if own is None else own).astype(F32)
+        for g in range(1, groups):
+            added = added + recv[first + peer(g)].astype(F32)
+        return added
+
+    def send_proj(zone, cols=slice(0, wide)):
+        def send(slab, place, partner):
+            remote(
+                proj_send.at[slab, :, cols],
+                proj_recv.at[place, :, cols],
+                1,
+                plane_sem + zone,
+                partner,
+                1 - tp,
+            ).start()
+
+        for g in range(1, groups):
+            send(
+                zone * groups + peer(g),
+                zone * groups + group_me,
+                zone_me * groups + peer(g),
+            )
+        send(zone * groups + group_me, zone * groups + group_me, me)
+
+    for c in range(2):
+        loaded(v_proj.at[:, :, halves[c]], 3 + c)
+        parts = [
+            dot(low, v_proj[p, :, halves[c]]) + dot(high, v_proj[p + 1, :, halves[c]])
+            for p in (0, 2)
+        ]
+        parts = [part.reshape(kv_count, 2 * NEW, half) for part in parts]
+        proj_send[:, :, halves[c]] = jnp.concatenate(parts, axis=1).astype(BF16)
+        if c == 0:
+            pl.semaphore_wait(barrier, 2 * (groups + zones - 2) + 1)
+        send_proj(zone_of(steps[0]), halves[c])
+    load(memory, v_mem, 9).start()
+    load(w_output, v_output, 10).start()
+    load(w_gate, v_gu.at[0], 11).start()
+    load(w_up, v_gu.at[1], 11).start()
+    load(w_down, v_down, 12).start()
     loaded(v_ab, 2)
     w_small = (dot(one_alpha, v_ab[0]) + dot(one_beta, v_ab[1])).astype(BF16)
     small = jnp.zeros((kv_count, TILE), F32)
@@ -339,22 +395,6 @@
         )
     small_send[:, :, 0, :] = small.reshape(groups, zones, TILE)
     small_send[:, :, 1, :] = squares.reshape(groups, zones, TILE)
-    for c in range(2):
-        loaded(v_proj.at[:, :, halves[c]], 3 + c)
-        parts = [
-            dot(low, v_proj[p, :, halves[c]]) + dot(high, v_proj[p + 1, :, halves[c]])
-            for p in (0, 2)
-        ]
-        parts = [part.reshape(kv_count, 2 * NEW, half) for part in parts]
-        proj_send[:, :, halves[c]] = jnp.concatenate(parts, axis=1).astype(BF16)
-    load(memory, v_mem, 9).start()
-    load(w_output, v_output, 10).start()
-    load(w_gate, v_gu.at[0], 11).start()
-    load(w_up, v_gu.at[1], 11).start()
-    load(w_down, v_down, 12).start()
-
-    pl.semaphore_wait(barrier, groups + zones - 1)
-
     for g in range(1, groups):
         remote(
             small_send.at[peer(g)],
@@ -363,41 +403,16 @@
             small_sem,
             zone_me * groups + peer(g),
         ).start()
-
-    def send_plane(send, recv, sent, sem, zone):
-        for g in range(1, groups):
-            remote(
-                send.at[zone * groups + peer(g)],
-                recv.at[zone * groups + group_me],
-                sent,
-                sem + zone,
-                zone_me * groups + peer(g),
-            ).start()
-
-    def sum_plane(send, recv, sem, zone):
-        arrived(recv.at[pl.ds(zone * groups, groups - 1)], sem + zone)
-        added = send[zone * groups + group_me].astype(F32)
-        for g in range(1, groups):
-            added = added + recv[zone * groups + peer(g)].astype(F32)
-        return added
-
-    def reduce_start(send, recv, part, last, sem, sent, arrival):
-        for step in steps[:-1]:
-            zone = zone_of(step)
-            part[zone] = sum_plane(send, recv, sem, zone).astype(BF16)
-            remote(
-                part.at[zone], last.at[zone_me], sent, arrival, zone * groups + group_me
-            ).start()
-        return sum_plane(send, recv, sem, zone_me)
-
-    def reduce_end(added, last, arrival):
-        arrived(last.at[pl.ds(0, zones - 1)], arrival)
-        for step in steps[:-1]:
-            added = added + last[zone_of(step)].astype(F32)
-        return added
-
-    for step in steps:
-        send_plane(proj_send, proj_recv, 1, plane_sem, zone_of(step))
+    for step in steps[1:-1]:
+        send_proj(zone_of(step))
+    for g in range(1, groups):
+        remote(
+            proj_send.at[zone_me * groups + peer(g)],
+            proj_recv.at[me],
+            1,
+            plane_sem + zone_me,
+            zone_me * groups + peer(g),
+        ).start()
 
     loaded(lens, 5)
     loaded(decay_in, 6)
@@ -426,17 +441,33 @@
         start_c = jnp.where(seq_c == s, begin, start_c)
         begin = begin + lens[s]
     slot_a = iota(shape_a, 1) & 3
-    rank_a = jnp.where(slot_a < length_a, start_a + slot_a, -1)
+
+    def padded(rank):
+        return sum(((rank >= g * held).astype(jnp.int32) for g in range(1, groups)), rank)
+
+    rank_a = jnp.where(slot_a < length_a, padded(start_a + slot_a), -1)
     pack = jnp.where(rank_a == iota((compact, rows), 0), 1.0, 0.0).astype(BF16)
     slot_c = iota(shape_c, 0) & 3
-    rank_c = jnp.where(slot_c < length_c, start_c + slot_c, -1)
+    rank_c = jnp.where(slot_c < length_c, padded(start_c + slot_c), -1)
     unpack = jnp.where(rank_c == iota(shape_c, 1), 1.0, 0.0).astype(BF16)
     slot_b = iota(shape_b, 1) & 3
     head_b = (iota(shape_b, 1) >> 2) & (heads - 1)
-    rank_b = jnp.where(slot_b < length_b, head_b * compact + start_b + slot_b, -1)
+    rank_b = jnp.where(slot_b < length_b, head_b * compact + padded(start_b + slot_b), -1)
     collect = jnp.where(rank_b == iota((heads * compact, slots_wide), 0), 1.0, 0.0).astype(BF16)
     tok_packed = dot(pack, tok)
 
+    def proj_onward(zone):
+        proj_part[zone] = sum_plane(proj_recv, plane_sem + zone, zone * groups, None).astype(BF16)
+        remote(
+            proj_part.at[zone],
+            proj_last.at[zone_me],
+            3,
+            proj_sem,
+            zone * groups + group_me,
+            1 - tp,
+        ).start()
+
+    proj_onward(zone_of(steps[0]))
     arrived(small_recv.at[pl.ds(0, groups - 1)], small_sem)
     small = small_send[group_me]
     for g in range(1, groups):
@@ -448,7 +479,9 @@
             small_part.at[zone], small_last.at[zone_me], 2, few_sem, zone * groups + group_me
         ).start()
 
-    total = reduce_start(proj_send, proj_recv, proj_part, proj_last, plane_sem, 3, proj_sem)
+    for step in steps[1:-1]:
+        proj_onward(zone_of(step))
+    total = sum_plane(proj_recv, plane_sem + zone_me, zone_me * groups, proj_send[me])
     arrived(small_last.at[pl.ds(0, zones - 1)], few_sem)
     small = small_part[zone_me]
     for step in steps[:-1]:
@@ -480,7 +513,9 @@
         decay.append(jnp.exp(jnp.where(live, -rate * soft, 0.0)))
         beta.append(jnp.where(live, jax.nn.sigmoid(write), 0.0))
     loaded(v_mem, 9)
-    total = reduce_end(total, proj_last, proj_sem)
+    arrived(proj_last.at[pl.ds(0, zones - 1)], proj_sem)
+    for step in steps[:-1]:
+        total = total + proj_last[zone_of(step)].astype(F32)
     scale = rs_buf[...]
     for h in range(heads):
         piece = total[:, h * DV : (h + 1) * DV] * scale
@@ -523,11 +558,14 @@
         mix_buf[pl.ds(t, heads, stride=NEW), :] = o
     mix_all[me] = mix_buf[...].astype(BF16)
 
-    @pl.loop(1, kv_count)
-    def _(off):
-        to = lax.rem(me + off, kv_count)
-        remote(mix_all.at[me], mix_all.at[me], 4, mix_sem, to).start()
-
+    def send_mix():
+        for step in steps:
+            for g in [*range(1, groups), 0]:
+                if step or g:
+                    to = zone_of(step) * groups + peer(g)
+                    remote(mix_all.at[me], mix_all.at[me], 4, mix_sem, to).start()
+
+    pl.when(tp == 0)(send_mix)
     u_buf[...] = jnp.zeros_like(u_buf)
     after = jnp.ones((heads, 1), F32)
     for t in range(NEW - 1, -1, -1):
@@ -543,6 +581,7 @@
             preferred_element_type=F32,
         )
         v_mem[h] = v_mem[h] * a_buf[h : h + 1, :] + outer
+    pl.when(tp == 1)(send_mix)
     loaded(v_output, 10)
     loaded(v_gu, 11)
     loaded(v_down, 12)
@@ -555,82 +594,197 @@
     )
     attended = tp_swap(0, dot(packed, v_output[...]))
     hidden = (tok_packed + attended).astype(BF16).astype(F32)
-    squares = jnp.sum(hidden * hidden, axis=1, keepdims=True)
-    spot = (iota((compact, TILE), 0) & (GROUP - 1)) == iota((compact, TILE), 1)
-    squares = jnp.sum(jnp.where(spot, squares, 0.0).reshape(groups, GROUP, TILE), axis=1)
-    sq_send[...] = squares.reshape(groups, 1, TILE)
-    sq_recv[me] = sq_send[group_me]
-
-    @pl.loop(1, kv_count)
-    def _(off):
-        to = lax.rem(me + off, kv_count)
-        remote(sq_send.at[lax.rem(to, groups)], sq_recv.at[me], 5, sq_sem, to).start()
 
     hscaled = hidden * mlp_gain[...]
     blank = jnp.zeros((GROUP, width), F32)
-    gate_rows, up_rows = [], []
+    gate_rows = []
     for g in range(groups):
-        own = hscaled[g * GROUP : (g + 1) * GROUP, :]
-        gate_rows += [own, blank]
-        up_rows += [blank, own]
-    gate_rows = jnp.concatenate(gate_rows, axis=0).astype(BF16)
-    up_rows = jnp.concatenate(up_rows, axis=0).astype(BF16)
+        gate_rows += [hscaled[g * GROUP : (g + 1) * GROUP, :], blank]
+    gate_rows = jnp.concatenate(gate_rows, axis=0)
+    up_rows = pltpu.roll(gate_rows, held, 0).astype(BF16)
+    gate_rows = gate_rows.astype(BF16)
+    spare = (iota((2 * compact, TILE), 0) & (2 * GROUP - 1)) >= 2 * held
     for step in steps:
         zone = zone_of(step)
         cols = pl.ds(pl.multiple_of(zone * chunk, TILE), chunk)
         term = dot(gate_rows, v_gu[0, :, cols]) + dot(up_rows, v_gu[1, :, cols])
+        last = term[:, sent:]
+        tiles = [
+            jnp.where(
+                spare,
+                pltpu.roll(last, 2 * (held - k), 0),
+                term[:, k * TILE : (k + 1) * TILE],
+            )
+            for k in range(held)
+        ]
+        term = jnp.concatenate([*tiles, term[:, held * TILE : sent]], axis=1)
         gu_send[pl.ds(zone * groups, groups)] = term.astype(BF16).reshape(
-            groups, 2 * GROUP, chunk
+            groups, 2 * GROUP, sent
         )
-        send_plane(gu_send, gu_recv, 6, gu_sem, zone)
-    both = reduce_start(gu_send, gu_recv, gu_part, gu_last, gu_sem, 7, mlp_sem)
-    arrived(sq_recv.at[pl.ds(0, kv_count - 1)], sq_sem)
-    mean_sq = jnp.sum(sq_recv[...].reshape(kv_count, TILE), axis=0, keepdims=True)
-    spot = iota((GROUP, TILE), 0) == iota((GROUP, TILE), 1)
-    mean_sq = jnp.sum(jnp.where(spot, mean_sq, 0.0), axis=1, keepdims=True)
-    rstd2 = lax.rsqrt(mean_sq / total_width + epsilon)
-    both = reduce_end(both, gu_last, mlp_sem)
-    gated = both[:GROUP] * rstd2
-    active = gated * jax.nn.sigmoid(gated) * (both[GROUP:] * rstd2)
-    act_all[me] = active.astype(BF16)
-
-    def pass_on(zone, arrival, partner):
-        block = zone * groups + group_me
-        remote(act_all.at[block], act_all.at[block], 8, arrival, partner).start()
-
-    def forward(zone):
+        arrival = gu_sem + tp * zones + zone
         for g in range(1, groups):
-            pass_on(zone, far_sem + zone, zone_me * groups + peer(g))
-
-    for step in steps[:-1]:
-        pass_on(zone_me, near_sem + zone_me, zone_of(step) * groups + group_me)
-    forward(zone_me)
+            remote(
+                gu_send.at[zone * groups + peer(g)],
+                gu_recv.at[tp * kv_count + zone * groups + group_me],
+                6,
+                arrival,
+                zone_me * groups + peer(g),
+                1,
+            ).start()
+
+        @pl.when(tp == 0)
+        def _():
+            slab = zone * groups + group_me
+            remote(gu_send.at[slab], gu_recv.at[slab], 6, arrival, me, 1).start()
+
+        if step == steps[0]:
+
+            @pl.when(tp == 1)
+            def _():
+                squares = jnp.sum(hidden * hidden, axis=1, keepdims=True)
+                spot = (iota((compact, TILE), 0) & (GROUP - 1)) == iota((compact, TILE), 1)
+                squares = jnp.sum(jnp.where(spot, squares, 0.0).reshape(groups, GROUP, TILE), axis=1)
+                sq_send[...] = squares.reshape(groups, 1, TILE)
+                sq_recv[me] = sq_send[group_me]
+
+                @pl.loop(1, kv_count)
+                def _(off):
+                    to = lax.rem(me + off, kv_count)
+                    remote(sq_send.at[lax.rem(to, groups)], sq_recv.at[me], 5, sq_sem, to).start()
+
     near_first = steps[::-1]
-    for step in near_first[1:]:
-        zone = zone_of(step)
-        arrived(act_all.at[zone * groups + group_me], near_sem + zone)
-        forward(zone)
+
+    @pl.when(tp == 1)
+    def _():
+        def plane_total(zone, core):
+            slab = zone * groups
+            own = gu_send[slab + group_me] if core else None
+            return sum_plane(gu_recv, gu_sem + core * zones + zone, core * kv_count + slab, own)
+
+        for step in steps[:-1]:
+            zone = zone_of(step)
+            for core in (1, 0):
+                gu_part[core * zones + zone] = plane_total(zone, core).astype(BF16)
+                remote(
+                    gu_part.at[core * zones + zone],
+                    gu_last.at[core * zones + zone_me],
+                    7,
+                    mlp_sem if core else both_sem,
+                    zone * groups + group_me,
+                ).start()
+        arrived(sq_recv.at[pl.ds(0, kv_count - 1)], sq_sem)
+        mean_sq = jnp.sum(sq_recv[...].reshape(kv_count, TILE), axis=0, keepdims=True)
+        spot = iota((GROUP, TILE), 0) == iota((GROUP, TILE), 1)
+        mean_sq = jnp.sum(jnp.where(spot, mean_sq, 0.0), axis=1, keepdims=True)
+        rstd2 = lax.rsqrt(mean_sq / total_width + epsilon)
+
+        def pass_on(zone, core, sent, arrival, partner, there):
+            block = core * kv_count + zone * groups + group_me
+            remote(act_all.at[block], act_all.at[block], sent, arrival, partner, there).start()
+
+        def forward(zone, core):
+            for g in range(1, groups):
+                pass_on(zone, core, 9, far_sem + zone, zone_me * groups + peer(g), core)
+            if core == 0:
+                pass_on(zone, 0, 9, far_sem + zone, me, 0)
+
+        for core in (0, 1):
+            both = plane_total(zone_me, core)
+            arrived(
+                gu_last.at[pl.ds(core * zones, zones - 1)], mlp_sem if core else both_sem
+            )
+            for step in steps[:-1]:
+                both = both + gu_last[core * zones + zone_of(step)].astype(F32)
+            row = iota((2 * GROUP, TILE), 0)
+            last = jnp.zeros((2 * GROUP, TILE), F32)
+            for k in range(held):
+                tile = both[:, k * TILE : (k + 1) * TILE]
+                back = pltpu.roll(tile, 2 * GROUP - 2 * (held - k), 0)
+                last = jnp.where(row >> 1 == k, back, last)
+            both = jnp.concatenate([both, last], axis=1)
+            gated = both[:GROUP] * rstd2
+            lifted = pltpu.roll(both, 2 * GROUP - held, 0)[:GROUP] * rstd2
+            active = gated * jax.nn.sigmoid(gated) * lifted
+            row = iota((GROUP, TILE), 0)
+            last = active[:, sent:]
+            tiles = [
+                jnp.where(
+                    row == held,
+                    last if k == held else pltpu.roll(last, held - k, 0),
+                    active[:, k * TILE : (k + 1) * TILE],
+                )
+                for k in range(held)
+            ]
+            active = jnp.concatenate([*tiles, active[:, held * TILE : sent]], axis=1)
+            act_all[core * kv_count + me] = active.astype(BF16)
+            for step in steps[:-1]:
+                there = zone_of(step) * groups + group_me
+                pass_on(zone_me, core, 8, near_sem + core * zones + zone_me, there, 1)
+            forward(zone_me, core)
+        for step in near_first[1:]:
+            zone = zone_of(step)
+            for core in (0, 1):
+                block = core * kv_count + zone * groups + group_me
+                arrived(act_all.at[block], near_sem + core * zones + zone)
+                forward(zone, core)
+
     feed = jnp.zeros((compact, width), F32)
+    row_in = iota((compact, TILE), 0) & (GROUP - 1)
     for step in near_first:
         zone = zone_of(step)
-        arrived(act_all.at[pl.ds(zone * groups, groups - 1)], far_sem + zone)
-        part = act_all[pl.ds(zone * groups, groups)].astype(F32).reshape(compact, chunk)
+        first = tp * kv_count + zone * groups
+
+        @pl.when(tp == 0)
+        def _():
+            arrived(act_all.at[pl.ds(first, groups)], far_sem + zone)
+
+        @pl.when(tp == 1)
+        def _():
+            arrived(act_all.at[pl.ds(first, groups - 1)], far_sem + zone)
+
+        part = act_all[pl.ds(first, groups)].astype(F32).reshape(compact, sent)
+        last = jnp.zeros((compact, TILE), F32)
+        for k in range(held):
+            tile = part[:, k * TILE : (k + 1) * TILE]
+            last = jnp.where(row_in == k, pltpu.roll(tile, compact - (held - k), 0), last)
+        part = jnp.concatenate([part, last], axis=1)
         cols = pl.ds(pl.multiple_of(zone * chunk, TILE), chunk)
         feed = feed + dot(part.astype(BF16), v_down[cols, :])
 
     def drain():
         left(small_send.at[pl.ds(0, groups - 1)], 0)
-        left(proj_send.at[pl.ds(0, kv_count - zones)], 1)
+        left(proj_send.at[pl.ds(0, kv_count - 1)], 1)
         left(small_part.at[pl.ds(0, zones - 1)], 2)
         left(proj_part.at[pl.ds(0, zones - 1)], 3)
         left(mix_all.at[pl.ds(0, kv_count - 1)], 4)
-        left(sq_recv.at[pl.ds(0, kv_count - 1)], 5)
-        left(gu_send.at[pl.ds(0, kv_count - zones)], 6)
-        left(gu_part.at[pl.ds(0, zones - 1)], 7)
-        left(act_all.at[pl.ds(0, kv_count - 1)], 8)
-
-    result = (hidden + tp_swap(1, feed, drain)).astype(BF16)
+
+        @pl.when(tp == 0)
+        def _():
+            left(gu_send, 6)
+
+        @pl.when(tp == 1)
+        def _():
+            left(sq_recv.at[pl.ds(0, kv_count - 1)], 5)
+            left(gu_send.at[pl.ds(0, kv_count - zones)], 6)
+            left(gu_part.at[pl.ds(0, 2 * (zones - 1))], 7)
+            left(act_all.at[pl.ds(0, 2 * (zones - 1))], 8)
+            left(act_all.at[pl.ds(0, zones * (2 * groups - 1))], 9)
+
+    result = hidden + tp_swap(1, feed, drain)
+    result = jnp.where((iota((compact, width), 0) & (GROUP - 1)) < held, result, 0.0)
+    result = result.astype(BF16)
     out[...] = dot(unpack, result).astype(BF16)
+
+
+def settle(out, state, out_far, state_far, sem):
+    moves = [
+        pltpu.make_async_copy(state, state_far, sem.at[0]),
+        pltpu.make_async_copy(out, out_far, sem.at[1]),
+    ]
+    for move in moves:
+        move.start()
+    for move in moves:
+        move.wait()
 
 
 def fused_device(
@@ -661,7 +815,7 @@
     compact = -(-live_rows // 16) * 16
     groups = compact // GROUP
     zones = kv_count // groups
-    chunk = w_gate.shape[1] // zones
+    sent = w_gate.shape[1] // zones - TILE
     wide = heads * DV
     near = pl.BlockSpec(memory_space=pltpu.VMEM)
     far = pl.BlockSpec(memory_space=pltpu.HBM)
@@ -705,14 +859,14 @@
             pltpu.VMEM((2, compact, width), F32),
             pltpu.VMEM((groups, 1, TILE), F32),
             pltpu.VMEM((kv_count, 1, TILE), F32),
-            pltpu.VMEM((kv_count, 2 * GROUP, chunk), BF16),
-            pltpu.VMEM((kv_count, 2 * GROUP, chunk), BF16),
-            pltpu.VMEM((zones, 2 * GROUP, chunk), BF16),
-            pltpu.VMEM((zones, 2 * GROUP, chunk), BF16),
-            pltpu.VMEM((kv_count, GROUP, chunk), BF16),
+            pltpu.VMEM((kv_count, 2 * GROUP, sent), BF16),
+            pltpu.VMEM((2 * kv_count, 2 * GROUP, sent), BF16),
+            pltpu.VMEM((2 * zones, 2 * GROUP, sent), BF16),
+            pltpu.VMEM((2 * zones, 2 * GROUP, sent), BF16),
+            pltpu.VMEM((2 * kv_count, GROUP, sent), BF16),
             pltpu.SemaphoreType.DMA((13,)),
-            pltpu.SemaphoreType.DMA((9,)),
-            pltpu.SemaphoreType.DMA((4 * zones + 6,)),
+            pltpu.SemaphoreType.DMA((10,)),
+            pltpu.SemaphoreType.DMA((6 * zones + 7,)),
             pltpu.SemaphoreType.DMA((2, 2)),
         ],
         compiler_params=pltpu.CompilerParams(
@@ -738,6 +892,17 @@
         w_up,
         w_down,
     )])
+    near = pl.BlockSpec(memory_space=pltpu.VMEM)
+    out, state = pl.pallas_call(
+        settle,
+        out_shape=(
+            jax.ShapeDtypeStruct(out.shape, out.dtype),
+            jax.ShapeDtypeStruct(state.shape, state.dtype),
+        ),
+        in_specs=[near] * 2,
+        out_specs=(far, far),
+        scratch_shapes=[pltpu.SemaphoreType.DMA((2,))],
+    )(*[pltpu.with_memory_space_constraint(x, pltpu.VMEM) for x in (out, state)])
     return out, state.reshape(memory.shape)
 
 
@@ -757,6 +922,8 @@
         and kv_count % groups == 0
         and w_gate.shape[1] % (kv_count // groups * TILE) == 0
         and NEW * 2 * all_heads == TILE
+        and live_rows == groups * (GROUP - 1)
+        and w_gate.shape[1] >= kv_count // groups * GROUP * TILE
     )
 
 

time: 46.8 us -> 44.3 us (0.947)
  local copies, waits for them, and re-layouts: 1.41 us -> 0 us
  Pallas kernels: 44.6 us -> 43.5 us
    pallas_call x1, Pallas kernels: 44.6 us -> 42.7 us  [fused_device(): pl.pallas_call(fused, out_shape=(jax.ShapeDtypeStruct((rows, width), BF16...]
    unnamed x2 -> x0, local copies, waits for them, and re-layouts: 1.41 us -> none
    pallas_call x0 -> x1, Pallas kernels: none -> 0.81 us  [fused_device(): pl.pallas_call(settle, out_shape=(jax.ShapeDtypeStruct(out.shape, out.dty...]
where the time goes in v2:
time: 44.3 us; the launch traced here: 44.2 us
  Pallas kernels  43.5 us (98%)
  between operations  0.65 us (1%)
    pallas_call x1, Pallas kernels, fused_device(): pl.pallas_call(fused, out_shape=(jax.ShapeDtypeStruct((rows, width), BF16...  42.7 us

profile of v2, /device:TPU:0, one launch (start us, length us, event | category | flops | bytes accessed | tf_op | source)
XLA Modules:
  0.0 44.2 jit_solution(10435597005348936395)
XLA Ops:
  0.6 42.7 %shard_map.185 = (bf16[64,256]{1,0:T(8,128)(2,1)S(1)}, f32[8,128,128]{2,1,0:T(8,128)S(1)}) custom-call(s32[16]{0:T(128)} %lens_far.1, bf16[64,256]{1,0:T(8,128)(2,1)} %tokens_far.1, f32[1,256]{1,0:T(1,128)} %bitcast.12, f32[1,8]{1,0:T(1,128)} %bitcast.14, f32[1,8]{1,0:T(1,128)} %bitcast.15, f32[1,128]{1,0:T(1,128)} %bitcast.16, f32[1,256]{1,0:T(1,128)} %bitcast.13, ...), custom_call_target="tpu_custom_call" | custom-call | tf_op jit(solution)/shard_map/pallas_call | solution.py:822
  43.3 0.8 %shard_map.186 = (bf16[64,256]{1,0:T(8,128)(2,1)}, f32[8,128,128]{2,1,0:T(8,128)}) custom-call(bf16[64,256]{1,0:T(8,128)(2,1)S(1)} %get-tuple-element.6.out, f32[8,128,128]{2,1,0:T(8,128)S(1)} %get-tuple-element.7.state), custom_call_target="tpu_custom_call" | custom-call | tf_op jit(solution)/shard_map/pallas_call | solution.py:896

commit v3 on v2

--- a/solution.py
+++ b/solution.py
@@ -179,6 +179,9 @@
     proj_recv,
     proj_part,
     proj_last,
+    pf_recv,
+    pf_part,
+    pf_last,
     small_send,
     small_recv,
     small_part,
@@ -199,6 +202,9 @@
     gu_recv,
     gu_part,
     gu_last,
+    zf_recv,
+    zf_part,
+    zf_last,
     act_all,
     load_sem,
     send_sem,
@@ -217,6 +223,8 @@
     sent = gu_send.shape[2]
     chunk = sent + TILE
     held = GROUP - 1
+    main = gu_recv.shape[2]
+    wide_main = proj_recv.shape[2]
     total_width = width * kv_count
     all_heads = v_ab.shape[1]
     zone_me = me // groups
@@ -227,8 +235,12 @@
     def zone_of(step):
         if zones != 4:
             return lax.rem(zone_me + step, zones)
-        across = (1 - side) * 2
-        return [zone_me, across + 1 - odd, across + odd, side * 2 + 1 - odd][step]
+        end = 1 - (side - odd) * (side - odd)
+        far_end, near_end = (1 - side) * 3, side * 3
+        far_mid, near_mid = 2 - side, 1 + side
+        second = end * far_mid + (1 - end) * near_end
+        third = end * near_mid + (1 - end) * far_mid
+        return [zone_me, far_end, second, third][step]
 
     def peer(g):
         if groups != 4:
@@ -264,7 +276,7 @@
     load(norm_far, norm_gain, 1).start()
     load(alpha_far, v_ab.at[0], 2).start()
     load(beta_far, v_ab.at[1], 2).start()
-    for c in range(2):
+    for c in (1, 0):
         for p, weight in enumerate((w_query, w_key, w_value, w_outgate)):
             load(weight.at[:, halves[c]], v_proj.at[p, :, halves[c]], 3 + c).start()
     load(lens_far, lens, 5).start()
@@ -279,6 +291,8 @@
     plane_sem, gu_sem, near_sem, far_sem = 0, zones, 3 * zones, 5 * zones
     proj_sem, mlp_sem, mix_sem, small_sem, few_sem, sq_sem = range(6 * zones, 6 * zones + 6)
     both_sem = 6 * zones + 6
+    first_sem, then_sem = 6 * zones + 7, 6 * zones + 9
+    early_sem, onward_sem = 6 * zones + 11, 6 * zones + 12
 
     def remote(src, dst, sent, arrival, partner, core=None):
         return pltpu.make_async_remote_copy(
@@ -341,7 +355,7 @@
             added = added + recv[first + peer(g)].astype(F32)
         return added
 
-    def send_proj(zone, cols=slice(0, wide)):
+    def send_proj(zone, cols=slice(0, wide_main)):
         def send(slab, place, partner):
             remote(
                 proj_send.at[slab, :, cols],
@@ -360,7 +374,7 @@
             )
         send(zone * groups + group_me, zone * groups + group_me, me)
 
-    for c in range(2):
+    for c in (1, 0):
         loaded(v_proj.at[:, :, halves[c]], 3 + c)
         parts = [
             dot(low, v_proj[p, :, halves[c]]) + dot(high, v_proj[p + 1, :, halves[c]])
@@ -368,9 +382,19 @@
         ]
         parts = [part.reshape(kv_count, 2 * NEW, half) for part in parts]
         proj_send[:, :, halves[c]] = jnp.concatenate(parts, axis=1).astype(BF16)
-        if c == 0:
+        if c:
             pl.semaphore_wait(barrier, 2 * (groups + zones - 2) + 1)
-        send_proj(zone_of(steps[0]), halves[c])
+            for step in steps:
+                zone = zone_of(step)
+                remote(
+                    proj_send.at[pl.ds(zone * groups, groups), :, wide_main:],
+                    pf_recv.at[zone_me],
+                    12,
+                    early_sem,
+                    zone * groups + group_me,
+                    1 - tp,
+                ).start()
+        send_proj(zone_of(steps[0]), slice(c * half, wide_main if c else half))
     load(memory, v_mem, 9).start()
     load(w_output, v_output, 10).start()
     load(w_gate, v_gu.at[0], 11).start()
@@ -407,7 +431,7 @@
         send_proj(zone_of(step))
     for g in range(1, groups):
         remote(
-            proj_send.at[zone_me * groups + peer(g)],
+            proj_send.at[zone_me * groups + peer(g), :, :wide_main],
             proj_recv.at[me],
             1,
             plane_sem + zone_me,
@@ -479,9 +503,24 @@
             small_part.at[zone], small_last.at[zone_me], 2, few_sem, zone * groups + group_me
         ).start()
 
-    for step in steps[1:-1]:
+    proj_onward(zone_of(steps[1]))
+    arrived(pf_recv, early_sem)
+    early = pf_recv[0].astype(F32)
+    for zone in range(1, zones):
+        early = early + pf_recv[zone].astype(F32)
+    pf_part[...] = early.astype(BF16)
+    for g in [*range(1, groups), 0]:
+        remote(
+            pf_part.at[peer(g)],
+            pf_last.at[group_me],
+            13,
+            onward_sem,
+            zone_me * groups + peer(g),
+            1 - tp,
+        ).start()
+    for step in steps[2:-1]:
         proj_onward(zone_of(step))
-    total = sum_plane(proj_recv, plane_sem + zone_me, zone_me * groups, proj_send[me])
+    total = sum_plane(proj_recv, plane_sem + zone_me, zone_me * groups, proj_send[me, :, :wide_main])
     arrived(small_last.at[pl.ds(0, zones - 1)], few_sem)
     small = small_part[zone_me]
     for step in steps[:-1]:
@@ -516,6 +555,11 @@
     arrived(proj_last.at[pl.ds(0, zones - 1)], proj_sem)
     for step in steps[:-1]:
         total = total + proj_last[zone_of(step)].astype(F32)
+    arrived(pf_last, onward_sem)
+    early = pf_last[0].astype(F32)
+    for g in range(1, groups):
+        early = early + pf_last[g].astype(F32)
+    total = jnp.concatenate([total, early], axis=1)
     scale = rs_buf[...]
     for h in range(heads):
         piece = total[:, h * DV : (h + 1) * DV] * scale
@@ -565,7 +609,7 @@
                     to = zone_of(step) * groups + peer(g)
                     remote(mix_all.at[me], mix_all.at[me], 4, mix_sem, to).start()
 
-    pl.when(tp == 0)(send_mix)
+    send_mix()
     u_buf[...] = jnp.zeros_like(u_buf)
     after = jnp.ones((heads, 1), F32)
     for t in range(NEW - 1, -1, -1):
@@ -581,7 +625,6 @@
             preferred_element_type=F32,
         )
         v_mem[h] = v_mem[h] * a_buf[h : h + 1, :] + outer
-    pl.when(tp == 1)(send_mix)
     loaded(v_output, 10)
     loaded(v_gu, 11)
     loaded(v_down, 12)
@@ -624,7 +667,7 @@
         arrival = gu_sem + tp * zones + zone
         for g in range(1, groups):
             remote(
-                gu_send.at[zone * groups + peer(g)],
+                gu_send.at[zone * groups + peer(g), :, :main],
                 gu_recv.at[tp * kv_count + zone * groups + group_me],
                 6,
                 arrival,
@@ -632,10 +675,18 @@
                 1,
             ).start()
 
+        rest = gu_send.at[pl.ds(zone * groups, groups), :, main:]
+        lands = zf_recv.at[tp * zones + zone_me]
+        if step:
+            there = zone * groups + group_me
+            remote(rest, lands, 10, first_sem + tp, there, 1).start()
+
         @pl.when(tp == 0)
         def _():
             slab = zone * groups + group_me
-            remote(gu_send.at[slab], gu_recv.at[slab], 6, arrival, me, 1).start()
+            remote(gu_send.at[slab, :, :main], gu_recv.at[slab], 6, arrival, me, 1).start()
+            if not step:
+                remote(rest, lands, 10, first_sem, me, 1).start()
 
         if step == steps[0]:
 
@@ -658,8 +709,26 @@
     def _():
         def plane_total(zone, core):
             slab = zone * groups
-            own = gu_send[slab + group_me] if core else None
+            own = gu_send[slab + group_me, :, :main] if core else None
             return sum_plane(gu_recv, gu_sem + core * zones + zone, core * kv_count + slab, own)
+
+        def zones_total(core):
+            arrived(zf_recv.at[pl.ds(core * zones, zones - core)], first_sem + core)
+            if core:
+                added = gu_send[pl.ds(zone_me * groups, groups), :, main:].astype(F32)
+            else:
+                added = zf_recv[zone_me].astype(F32)
+            for step in steps[:-1]:
+                added = added + zf_recv[core * zones + zone_of(step)].astype(F32)
+            zf_part[pl.ds(core * groups, groups)] = added.astype(BF16)
+            for g in range(1, groups):
+                remote(
+                    zf_part.at[core * groups + peer(g)],
+                    zf_last.at[core * groups + group_me],
+                    11,
+                    then_sem + core,
+                    zone_me * groups + peer(g),
+                ).start()
 
         for step in steps[:-1]:
             zone = zone_of(step)
@@ -672,6 +741,9 @@
                     mlp_sem if core else both_sem,
                     zone * groups + group_me,
                 ).start()
+            if step == steps[1]:
+                for core in (1, 0):
+                    zones_total(core)
         arrived(sq_recv.at[pl.ds(0, kv_count - 1)], sq_sem)
         mean_sq = jnp.sum(sq_recv[...].reshape(kv_count, TILE), axis=0, keepdims=True)
         spot = iota((GROUP, TILE), 0) == iota((GROUP, TILE), 1)
@@ -695,6 +767,11 @@
             )
             for step in steps[:-1]:
                 both = both + gu_last[core * zones + zone_of(step)].astype(F32)
+            arrived(zf_last.at[pl.ds(core * groups, groups - 1)], then_sem + core)
+            apart = zf_part[core * groups + group_me].astype(F32)
+            for g in range(1, groups):
+                apart = apart + zf_last[core * groups + peer(g)].astype(F32)
+            both = jnp.concatenate([both, apart], axis=1)
             row = iota((2 * GROUP, TILE), 0)
             last = jnp.zeros((2 * GROUP, TILE), F32)
             for k in range(held):
@@ -753,19 +830,24 @@
 
     def drain():
         left(small_send.at[pl.ds(0, groups - 1)], 0)
-        left(proj_send.at[pl.ds(0, kv_count - 1)], 1)
+        left(proj_recv.at[pl.ds(0, kv_count - 1)], 1)
+        left(pf_recv, 12)
+        left(pf_last, 13)
         left(small_part.at[pl.ds(0, zones - 1)], 2)
         left(proj_part.at[pl.ds(0, zones - 1)], 3)
         left(mix_all.at[pl.ds(0, kv_count - 1)], 4)
 
         @pl.when(tp == 0)
         def _():
-            left(gu_send, 6)
+            left(gu_recv.at[pl.ds(0, kv_count)], 6)
+            left(zf_recv.at[pl.ds(0, zones)], 10)
 
         @pl.when(tp == 1)
         def _():
             left(sq_recv.at[pl.ds(0, kv_count - 1)], 5)
-            left(gu_send.at[pl.ds(0, kv_count - zones)], 6)
+            left(gu_recv.at[pl.ds(0, kv_count - zones)], 6)
+            left(zf_recv.at[pl.ds(0, zones - 1)], 10)
+            left(zf_last.at[pl.ds(0, 2 * (groups - 1))], 11)
             left(gu_part.at[pl.ds(0, 2 * (zones - 1))], 7)
             left(act_all.at[pl.ds(0, 2 * (zones - 1))], 8)
             left(act_all.at[pl.ds(0, zones * (2 * groups - 1))], 9)
@@ -816,7 +898,9 @@
     groups = compact // GROUP
     zones = kv_count // groups
     sent = w_gate.shape[1] // zones - TILE
+    main = sent - 2 * TILE
     wide = heads * DV
+    early = 2 * TILE
     near = pl.BlockSpec(memory_space=pltpu.VMEM)
     far = pl.BlockSpec(memory_space=pltpu.HBM)
     out, state = pl.pallas_call(
@@ -840,9 +924,12 @@
             pltpu.VMEM((2, *w_gate.shape), BF16),
             pltpu.VMEM(w_down.shape, BF16),
             pltpu.VMEM((kv_count, 16, wide), BF16),
-            pltpu.VMEM((kv_count, 16, wide), BF16),
-            pltpu.VMEM((zones, 16, wide), BF16),
-            pltpu.VMEM((zones, 16, wide), BF16),
+            pltpu.VMEM((kv_count, 16, wide - early), BF16),
+            pltpu.VMEM((zones, 16, wide - early), BF16),
+            pltpu.VMEM((zones, 16, wide - early), BF16),
+            pltpu.VMEM((zones, groups, 16, early), BF16),
+            pltpu.VMEM((groups, 16, early), BF16),
+            pltpu.VMEM((groups, 16, early), BF16),
             pltpu.VMEM((groups, zones, 2, TILE), F32),
             pltpu.VMEM((groups, zones, 2, TILE), F32),
             pltpu.VMEM((zones, 2, TILE), F32),
@@ -860,13 +947,16 @@
             pltpu.VMEM((groups, 1, TILE), F32),
             pltpu.VMEM((kv_count, 1, TILE), F32),
             pltpu.VMEM((kv_count, 2 * GROUP, sent), BF16),
-            pltpu.VMEM((2 * kv_count, 2 * GROUP, sent), BF16),
-            pltpu.VMEM((2 * zones, 2 * GROUP, sent), BF16),
-            pltpu.VMEM((2 * zones, 2 * GROUP, sent), BF16),
+            pltpu.VMEM((2 * kv_count, 2 * GROUP, main), BF16),
+            pltpu.VMEM((2 * zones, 2 * GROUP, main), BF16),
+            pltpu.VMEM((2 * zones, 2 * GROUP, main), BF16),
+            pltpu.VMEM((2 * zones, groups, 2 * GROUP, sent - main), BF16),
+            pltpu.VMEM((2 * groups, 2 * GROUP, sent - main), BF16),
+            pltpu.VMEM((2 * groups, 2 * GROUP, sent - main), BF16),
             pltpu.VMEM((2 * kv_count, GROUP, sent), BF16),
             pltpu.SemaphoreType.DMA((13,)),
-            pltpu.SemaphoreType.DMA((10,)),
-            pltpu.SemaphoreType.DMA((6 * zones + 7,)),
+            pltpu.SemaphoreType.DMA((14,)),
+            pltpu.SemaphoreType.DMA((6 * zones + 13,)),
             pltpu.SemaphoreType.DMA((2, 2)),
         ],
         compiler_params=pltpu.CompilerParams(

time: 44.3 us -> 41.2 us (0.930)
  Pallas kernels: 43.5 us -> 40.4 us
    pallas_call x1, Pallas kernels: 42.7 us -> 39.5 us  [fused_device(): pl.pallas_call(fused, out_shape=(jax.ShapeDtypeStruct((rows, width), BF16...]
where the time goes in v3:
time: 41.2 us; the launch traced here: 41 us
  Pallas kernels  40.4 us (98%)
  between operations  0.65 us (2%)
    pallas_call x1, Pallas kernels, fused_device(): pl.pallas_call(fused, out_shape=(jax.ShapeDtypeStruct((rows, width), BF16...  39.5 us

profile of v3, /device:TPU:0, one launch (start us, length us, event | category | flops | bytes accessed | tf_op | source)
XLA Modules:
  0.0 41.0 jit_solution(18248415517046960217)
XLA Ops:
  0.6 39.5 %shard_map.185 = (bf16[64,256]{1,0:T(8,128)(2,1)S(1)}, f32[8,128,128]{2,1,0:T(8,128)S(1)}) custom-call(s32[16]{0:T(128)} %lens_far.1, bf16[64,256]{1,0:T(8,128)(2,1)} %tokens_far.1, f32[1,256]{1,0:T(1,128)} %bitcast.12, f32[1,8]{1,0:T(1,128)} %bitcast.14, f32[1,8]{1,0:T(1,128)} %bitcast.15, f32[1,128]{1,0:T(1,128)} %bitcast.16, f32[1,256]{1,0:T(1,128)} %bitcast.13, ...), custom_call_target="tpu_custom_call" | custom-call | tf_op jit(solution)/shard_map/pallas_call | solution.py:906
  40.2 0.8 %shard_map.186 = (bf16[64,256]{1,0:T(8,128)(2,1)}, f32[8,128,128]{2,1,0:T(8,128)}) custom-call(bf16[64,256]{1,0:T(8,128)(2,1)S(1)} %get-tuple-element.6.out, f32[8,128,128]{2,1,0:T(8,128)S(1)} %get-tuple-element.7.state), custom_call_target="tpu_custom_call" | custom-call | tf_op jit(solution)/shard_map/pallas_call | solution.py:986

commit v4 on v3

--- a/solution.py
+++ b/solution.py
@@ -173,6 +173,7 @@
     v_ab,
     v_proj,
     v_output,
+    v_other,
     v_gu,
     v_down,
     proj_send,
@@ -189,6 +190,7 @@
     rs_buf,
     xs_buf,
     kq_buf,
+    m_split,
     r_buf,
     u_buf,
     a_buf,
@@ -211,7 +213,7 @@
     recv_sem,
     tp_sem,
 ):
-    kv_count = mix_all.shape[0]
+    kv_count = mix_all.shape[0] // 2
     me = lax.axis_index("kv")
     tp = lax.axis_index("tp")
     rows, width = tokens.shape
@@ -270,15 +272,16 @@
     def load(src, dst, sem):
         return pltpu.make_async_copy(src, dst, load_sem.at[sem])
 
-    half = wide // 2
-    halves = [slice(c * half, (c + 1) * half) for c in range(2)]
+    part_wide = wide - wide_main
+    pieces = wide // part_wide
+    spans = [slice(c * part_wide, (c + 1) * part_wide) for c in range(pieces)][::-1]
     load(tokens_far, tokens, 0).start()
     load(norm_far, norm_gain, 1).start()
     load(alpha_far, v_ab.at[0], 2).start()
     load(beta_far, v_ab.at[1], 2).start()
-    for c in (1, 0):
+    for c, span in enumerate(spans):
         for p, weight in enumerate((w_query, w_key, w_value, w_outgate)):
-            load(weight.at[:, halves[c]], v_proj.at[p, :, halves[c]], 3 + c).start()
+            load(weight.at[:, span], v_proj.at[p, :, span], 13 + c).start()
     load(lens_far, lens, 5).start()
     load(decay_log_far, decay_in.at[0], 6).start()
     load(decay_bias_far, decay_in.at[1], 6).start()
@@ -293,6 +296,7 @@
     both_sem = 6 * zones + 6
     first_sem, then_sem = 6 * zones + 7, 6 * zones + 9
     early_sem, onward_sem = 6 * zones + 11, 6 * zones + 12
+    mixed_sem, other_sem = 6 * zones + 13, 6 * zones + 14
 
     def remote(src, dst, sent, arrival, partner, core=None):
         return pltpu.make_async_remote_copy(
@@ -374,27 +378,27 @@
             )
         send(zone * groups + group_me, zone * groups + group_me, me)
 
-    for c in (1, 0):
-        loaded(v_proj.at[:, :, halves[c]], 3 + c)
+    for c, span in enumerate(spans):
+        loaded(v_proj.at[:, :, span], 13 + c)
         parts = [
-            dot(low, v_proj[p, :, halves[c]]) + dot(high, v_proj[p + 1, :, halves[c]])
-            for p in (0, 2)
+            dot(low, v_proj[p, :, span]) + dot(high, v_proj[p + 1, :, span]) for p in (0, 2)
         ]
-        parts = [part.reshape(kv_count, 2 * NEW, half) for part in parts]
-        proj_send[:, :, halves[c]] = jnp.concatenate(parts, axis=1).astype(BF16)
-        if c:
+        parts = [part.reshape(kv_count, 2 * NEW, part_wide) for part in parts]
+        proj_send[:, :, span] = jnp.concatenate(parts, axis=1).astype(BF16)
+        if c == 0:
             pl.semaphore_wait(barrier, 2 * (groups + zones - 2) + 1)
             for step in steps:
                 zone = zone_of(step)
                 remote(
-                    proj_send.at[pl.ds(zone * groups, groups), :, wide_main:],
+                    proj_send.at[pl.ds(zone * groups, groups), :, span],
                     pf_recv.at[zone_me],
                     12,
                     early_sem,
                     zone * groups + group_me,
                     1 - tp,
                 ).start()
-        send_proj(zone_of(steps[0]), slice(c * half, wide_main if c else half))
+        else:
+            send_proj(zone_of(steps[0]), span)
     load(memory, v_mem, 9).start()
     load(w_output, v_output, 10).start()
     load(w_gate, v_gu.at[0], 11).start()
@@ -491,6 +495,11 @@
             1 - tp,
         ).start()
 
+    loaded(v_mem, 9)
+    for h in range(heads):
+        m_high = v_mem[h].astype(BF16)
+        m_split[h, :, :DV] = m_high
+        m_split[h, :, DV:] = (v_mem[h] - m_high.astype(F32)).astype(BF16)
     proj_onward(zone_of(steps[0]))
     arrived(small_recv.at[pl.ds(0, groups - 1)], small_sem)
     small = small_send[group_me]
@@ -551,7 +560,6 @@
         live = own_length > t
         decay.append(jnp.exp(jnp.where(live, -rate * soft, 0.0)))
         beta.append(jnp.where(live, jax.nn.sigmoid(write), 0.0))
-    loaded(v_mem, 9)
     arrived(proj_last.at[pl.ds(0, zones - 1)], proj_sem)
     for step in steps[:-1]:
         total = total + proj_last[zone_of(step)].astype(F32)
@@ -577,7 +585,10 @@
         kq_buf[pl.ds(t, heads, stride=8), :] = key_rows[t]
         kq_buf[pl.ds(NEW + t, heads, stride=8), :] = query[t]
     for h in range(heads):
-        r_buf[h * 8 : (h + 1) * 8, :] = dot(kq_buf[h * 8 : (h + 1) * 8, :], v_mem[h], HIGH)
+        kq = kq_buf[h * 8 : (h + 1) * 8, :]
+        kq_high = kq.astype(BF16).astype(F32)
+        both = dot(jnp.concatenate([kq_high, kq - kq_high], axis=0).astype(BF16), m_split[h])
+        r_buf[h * 8 : (h + 1) * 8, :] = both[:8, :DV] + both[8:, :DV] + both[:8, DV:]
     seen_k = [slot_rows(r_buf, t, 8) for t in range(NEW)]
     seen_q = [slot_rows(r_buf, NEW + t, 8) for t in range(NEW)]
 
@@ -600,16 +611,26 @@
         o = o * lax.rsqrt(jnp.mean(o * o, axis=1, keepdims=True) + epsilon)
         o = o * head_gain[...] * (gate[t] * jax.nn.sigmoid(gate[t]))
         mix_buf[pl.ds(t, heads, stride=NEW), :] = o
-    mix_all[me] = mix_buf[...].astype(BF16)
+    own_mix = tp * kv_count + me
+    mix_all[own_mix] = mix_buf[...].astype(BF16)
 
     def send_mix():
         for step in steps:
             for g in [*range(1, groups), 0]:
                 if step or g:
                     to = zone_of(step) * groups + peer(g)
-                    remote(mix_all.at[me], mix_all.at[me], 4, mix_sem, to).start()
+                    block = mix_all.at[own_mix]
+                    remote(block, block, 4, mix_sem + tp * (mixed_sem - mix_sem), to, 1).start()
 
     send_mix()
+    loaded(v_output, 10)
+
+    @pl.when(tp == 0)
+    def _():
+        block = mix_all.at[own_mix]
+        remote(block, block, 4, mix_sem, me, 1).start()
+        remote(v_output, v_other, 14, other_sem, me, 1).start()
+
     u_buf[...] = jnp.zeros_like(u_buf)
     after = jnp.ones((heads, 1), F32)
     for t in range(NEW - 1, -1, -1):
@@ -625,17 +646,37 @@
             preferred_element_type=F32,
         )
         v_mem[h] = v_mem[h] * a_buf[h : h + 1, :] + outer
-    loaded(v_output, 10)
     loaded(v_gu, 11)
     loaded(v_down, 12)
-
-    arrived(mix_all.at[pl.ds(0, kv_count - 1)], mix_sem)
-    gathered = mix_all[...].reshape(slots_wide, DV)
-    packed = dot(collect, gathered).astype(BF16)
-    packed = jnp.concatenate(
-        [packed[h * compact : (h + 1) * compact, :] for h in range(heads)], axis=1
+    share = pltpu.make_async_remote_copy(
+        src_ref=tp_recv.at[0],
+        dst_ref=tp_recv.at[0],
+        send_sem=tp_sem.at[0, 0],
+        recv_sem=tp_sem.at[0, 1],
+        device_id={"tp": 1 - tp},
+        device_id_type=pl.DeviceIdType.MESH,
     )
-    attended = tp_swap(0, dot(packed, v_output[...]))
+
+    @pl.when(tp == 1)
+    def _():
+        def projected(core, weight):
+            gathered = mix_all[pl.ds(core * kv_count, kv_count)].reshape(slots_wide, DV)
+            packed = dot(collect, gathered).astype(BF16)
+            packed = [packed[h * compact : (h + 1) * compact, :] for h in range(heads)]
+            return dot(jnp.concatenate(packed, axis=1), weight[...])
+
+        arrived(v_other, other_sem)
+        arrived(mix_all.at[pl.ds(0, kv_count - 1)], mixed_sem)
+        attended = projected(1, v_output)
+        arrived(mix_all.at[pl.ds(0, kv_count)], mix_sem)
+        tp_recv[0] = attended + projected(0, v_other)
+        share.start()
+
+    @pl.when(tp == 0)
+    def _():
+        share.wait_recv()
+
+    attended = tp_recv[0]
     hidden = (tok_packed + attended).astype(BF16).astype(F32)
 
     hscaled = hidden * mlp_gain[...]
@@ -647,11 +688,30 @@
     up_rows = pltpu.roll(gate_rows, held, 0).astype(BF16)
     gate_rows = gate_rows.astype(BF16)
     spare = (iota((2 * compact, TILE), 0) & (2 * GROUP - 1)) >= 2 * held
+    def product(zone, start, count):
+        cols = pl.ds(pl.multiple_of(zone * chunk + start, TILE), count)
+        return dot(gate_rows, v_gu[0, :, cols]) + dot(up_rows, v_gu[1, :, cols])
+
+    def early_piece(turn):
+        zone = zone_of(turn)
+        piece = product(zone, main, sent - main).astype(BF16)
+        here = pl.ds(zone * groups, groups)
+        gu_send[here, :, main:] = piece.reshape(groups, 2 * GROUP, sent - main)
+        rest = gu_send.at[here, :, main:]
+        lands = zf_recv.at[tp * zones + zone_me]
+        if turn:
+            there = zone * groups + group_me
+            remote(rest, lands, 10, first_sem + tp, there, 1).start()
+        else:
+
+            @pl.when(tp == 0)
+            def _():
+                remote(rest, lands, 10, first_sem, me, 1).start()
+
     for step in steps:
         zone = zone_of(step)
-        cols = pl.ds(pl.multiple_of(zone * chunk, TILE), chunk)
-        term = dot(gate_rows, v_gu[0, :, cols]) + dot(up_rows, v_gu[1, :, cols])
-        last = term[:, sent:]
+        term = product(zone, 0, main)
+        last = product(zone, sent, TILE)
         tiles = [
             jnp.where(
                 spare,
@@ -660,9 +720,9 @@
             )
             for k in range(held)
         ]
-        term = jnp.concatenate([*tiles, term[:, held * TILE : sent]], axis=1)
-        gu_send[pl.ds(zone * groups, groups)] = term.astype(BF16).reshape(
-            groups, 2 * GROUP, sent
+        term = jnp.concatenate([*tiles, term[:, held * TILE : main]], axis=1)
+        gu_send[pl.ds(zone * groups, groups), :, :main] = term.astype(BF16).reshape(
+            groups, 2 * GROUP, main
         )
         arrival = gu_sem + tp * zones + zone
         for g in range(1, groups):
@@ -675,18 +735,14 @@
                 1,
             ).start()
 
-        rest = gu_send.at[pl.ds(zone * groups, groups), :, main:]
-        lands = zf_recv.at[tp * zones + zone_me]
-        if step:
-            there = zone * groups + group_me
-            remote(rest, lands, 10, first_sem + tp, there, 1).start()
-
         @pl.when(tp == 0)
         def _():
             slab = zone * groups + group_me
             remote(gu_send.at[slab, :, :main], gu_recv.at[slab], 6, arrival, me, 1).start()
-            if not step:
-                remote(rest, lands, 10, first_sem, me, 1).start()
+
+        if step == steps[1]:
+            for turn in steps:
+                early_piece(turn)
 
         if step == steps[0]:
 
@@ -732,7 +788,7 @@
 
         for step in steps[:-1]:
             zone = zone_of(step)
-            for core in (1, 0):
+            for core in (0, 1):
                 gu_part[core * zones + zone] = plane_total(zone, core).astype(BF16)
                 remote(
                     gu_part.at[core * zones + zone],
@@ -835,15 +891,18 @@
         left(pf_last, 13)
         left(small_part.at[pl.ds(0, zones - 1)], 2)
         left(proj_part.at[pl.ds(0, zones - 1)], 3)
-        left(mix_all.at[pl.ds(0, kv_count - 1)], 4)
 
         @pl.when(tp == 0)
         def _():
+            left(mix_all.at[pl.ds(0, kv_count)], 4)
+            left(v_other, 14)
             left(gu_recv.at[pl.ds(0, kv_count)], 6)
             left(zf_recv.at[pl.ds(0, zones)], 10)
 
         @pl.when(tp == 1)
         def _():
+            share.wait_send()
+            left(mix_all.at[pl.ds(0, kv_count - 1)], 4)
             left(sq_recv.at[pl.ds(0, kv_count - 1)], 5)
             left(gu_recv.at[pl.ds(0, kv_count - zones)], 6)
             left(zf_recv.at[pl.ds(0, zones - 1)], 10)
@@ -921,6 +980,7 @@
             pltpu.VMEM((2, all_heads, width), BF16),
             pltpu.VMEM((4, *w_query.shape), BF16),
             pltpu.VMEM(w_output.shape, BF16),
+            pltpu.VMEM(w_output.shape, BF16),
             pltpu.VMEM((2, *w_gate.shape), BF16),
             pltpu.VMEM(w_down.shape, BF16),
             pltpu.VMEM((kv_count, 16, wide), BF16),
@@ -937,11 +997,12 @@
             pltpu.VMEM((16, TILE), F32),
             pltpu.VMEM((heads * 16, TILE), F32),
             pltpu.VMEM((heads * 8, TILE), F32),
+            pltpu.VMEM((heads, DK, 2 * DV), BF16),
             pltpu.VMEM((heads * 8, TILE), F32),
             pltpu.VMEM((heads * 8, TILE), F32),
             pltpu.VMEM((heads, TILE), F32),
             pltpu.VMEM((heads * NEW, TILE), F32),
-            pltpu.VMEM((kv_count, heads * NEW, TILE), BF16),
+            pltpu.VMEM((2 * kv_count, heads * NEW, TILE), BF16),
             pltpu.VMEM((2, compact, width), F32),
             pltpu.VMEM((2, compact, width), F32),
             pltpu.VMEM((groups, 1, TILE), F32),
@@ -954,9 +1015,9 @@
             pltpu.VMEM((2 * groups, 2 * GROUP, sent - main), BF16),
             pltpu.VMEM((2 * groups, 2 * GROUP, sent - main), BF16),
             pltpu.VMEM((2 * kv_count, GROUP, sent), BF16),
-            pltpu.SemaphoreType.DMA((13,)),
-            pltpu.SemaphoreType.DMA((14,)),
-            pltpu.SemaphoreType.DMA((6 * zones + 13,)),
+            pltpu.SemaphoreType.DMA((13 + wide // early,)),
+            pltpu.SemaphoreType.DMA((15,)),
+            pltpu.SemaphoreType.DMA((6 * zones + 15,)),
             pltpu.SemaphoreType.DMA((2, 2)),
         ],
         compiler_params=pltpu.CompilerParams(

time: 41.2 us -> 40 us (0.971)
  Pallas kernels: 40.4 us -> 39.2 us
    pallas_call x1, Pallas kernels: 39.5 us -> 38.4 us  [fused_device(): pl.pallas_call(fused, out_shape=(jax.ShapeDtypeStruct((rows, width), BF16...]
where the time goes in v4:
time: 40 us; the launch traced here: 39.9 us
  Pallas kernels  39.2 us (98%)
  between operations  0.65 us (2%)
    pallas_call x1, Pallas kernels, fused_device(): pl.pallas_call(fused, out_shape=(jax.ShapeDtypeStruct((rows, width), BF16...  38.4 us
    pallas_call x1, Pallas kernels, fused_device(): pl.pallas_call(settle, out_shape=(jax.ShapeDtypeStruct(out.shape, out.dty...  0.81 us

profile of v4, /device:TPU:0, one launch (start us, length us, event | category | flops | bytes accessed | tf_op | source)
XLA Modules:
  0.0 39.9 jit_solution(2247874617646172644)
XLA Ops:
  0.6 38.4 %shard_map.185 = (bf16[64,256]{1,0:T(8,128)(2,1)S(1)}, f32[8,128,128]{2,1,0:T(8,128)S(1)}) custom-call(s32[16]{0:T(128)} %lens_far.1, bf16[64,256]{1,0:T(8,128)(2,1)} %tokens_far.1, f32[1,256]{1,0:T(1,128)} %bitcast.12, f32[1,8]{1,0:T(1,128)} %bitcast.14, f32[1,8]{1,0:T(1,128)} %bitcast.15, f32[1,128]{1,0:T(1,128)} %bitcast.16, f32[1,256]{1,0:T(1,128)} %bitcast.13, ...), custom_call_target="tpu_custom_call" | custom-call | tf_op jit(solution)/shard_map/pallas_call | solution.py:965
  39.1 0.8 %shard_map.186 = (bf16[64,256]{1,0:T(8,128)(2,1)}, f32[8,128,128]{2,1,0:T(8,128)}) custom-call(bf16[64,256]{1,0:T(8,128)(2,1)S(1)} %get-tuple-element.6.out, f32[8,128,128]{2,1,0:T(8,128)S(1)} %get-tuple-element.7.state), custom_call_target="tpu_custom_call" | custom-call | tf_op jit(solution)/shard_map/pallas_call | solution.py:1047
